TPU v7x, 32 devices: a whole 2x2x4 slice. The times are simulated.
32 devices in a mesh: ep: 4 (over y, x), tp: 8 (over z, core).
Axes of the slice: x: 2, y: 2, z: 4, core: 2. Of those that a mesh axis runs over, the one named last changes fastest.
Arguments:
- q_latent: bfloat16 [4096, 512], P('ep'), may hold values from -6 to 6
- kv_latent: bfloat16 [4096, 256], P('ep'), may hold values from -6 to 6
- rope_key: bfloat16 [4096, 32], P('ep'), may hold values from -1200 to 1200
- q_gain: float32 [512], replicated, may hold values from 0.1 to 1.9
- kv_gain: float32 [256], replicated, may hold values from 0.1 to 1.9
- w_query: bfloat16 [512, 1536], P(None, 'tp'), may hold values from -0.25 to 0.25
- w_keyval: bfloat16 [256, 2048], P(None, 'tp'), may hold values from -0.375 to 0.375
- w_output: bfloat16 [1024, 2048], P(None, 'tp'), may hold values from -0.1875 to 0.1875
- moe_input: bfloat16 [1024, 2048], P('ep'), may hold values from -6 to 6
- moe_gain: float32 [2048], replicated, may hold values from 0.1 to 1.9
- routes: int32 [1024, 2], P('ep'), may hold values from 0 to 3, all different within a row; in each aligned block of 32 rows (0 to 31, 32 to 63, ...) at most 24 rows name the same one
- route_weight: float32 [1024, 2], P('ep'), may hold values from 0.25 to 2
- expert_gate: bfloat16 [4, 2048, 4096], P('ep', None, 'tp'), may hold values from -0.125 to 0.125
- expert_up: bfloat16 [4, 2048, 4096], P('ep', None, 'tp'), may hold values from -0.125 to 0.125
- expert_down: bfloat16 [4, 4096, 2048], P('ep', 'tp'), may hold values from -0.09375 to 0.09375
- shared_gate: bfloat16 [2048, 2048], P(None, 'tp'), may hold values from -0.125 to 0.125
- shared_up: bfloat16 [2048, 2048], P(None, 'tp'), may hold values from -0.125 to 0.125
- shared_down: bfloat16 [2048, 2048], P('tp'), may hold values from -0.125 to 0.125
Outputs:
- mixed: bfloat16 [4096, 2048], P('ep', 'tp')
- moe_out: bfloat16 [1024, 2048], P(('ep', 'tp'))
Inputs may be any that keep to these rules, and one draw needn't show every extreme that they name: `routes`: in each aligned block of 32 rows (the rows of one device's output) no expert is named by more than 24 rows, a bound that some block reaches. Each row names 2 different experts.
All inputs are finite; a program needn't handle non-finite values.
Results may differ from a plain program's by a relative error of at most 0.023.
Values may be sent and summed in bfloat16 or wider, within the bound.
A program may use at most 128 MiB of HBM per device.

v0:
```python
import jax
import jax.numpy as jnp
import numpy as np
from jax import lax
from jax.experimental import pallas as pl
from jax.experimental.pallas import tpu as pltpu
from jax.sharding import PartitionSpec as P

NOPE = 64
ROPE_DIM = 32
VDIM = 64
MOE_DEV = 32


norm_eps = 1e-06
layer_eps = 1e-05
rotary_base = 10000.0
floor_value = -1e30


def rms_scale(values, gain):
    widened = values.astype(jnp.float32)
    return (
        widened * lax.rsqrt(jnp.mean(widened * widened, -1, keepdims=True) + norm_eps) * gain
    ).astype(jnp.bfloat16)


def layer_scale(values, gain):
    widened = values.astype(jnp.float32)
    centred = widened - jnp.mean(widened, -1, keepdims=True)
    return (
        centred * lax.rsqrt(jnp.mean(centred * centred, -1, keepdims=True) + layer_eps) * gain
    ).astype(jnp.bfloat16)


def rotary_tables(positions):
    halfway = ROPE_DIM // 2
    inverse = rotary_base ** (-(jnp.arange(halfway, dtype=jnp.float32) * 2.0 / ROPE_DIM))
    angles = positions.astype(jnp.float32)[:, None] * inverse[None, :]
    return (jnp.cos(angles), jnp.sin(angles))


def rotate(values, cosine_table, sine_table):
    halfway = values.shape[-1] // 2
    first_half = values[..., :halfway]
    second_half = values[..., halfway:]
    return jnp.concatenate(
        [
            first_half * cosine_table - second_half * sine_table,
            second_half * cosine_table + first_half * sine_table,
        ],
        -1,
    )


def block_stats(query_block, query_pos, keyvals, rotated_keys, key_pos):
    scale = float(NOPE + ROPE_DIM) ** (-0.5)
    scores = jnp.einsum(
        "qhd,khd->hqk",
        query_block[..., :NOPE],
        keyvals[..., :NOPE],
        preferred_element_type=jnp.float32,
    )
    scores = (
        scores
        + jnp.einsum(
            "qhd,kd->hqk", query_block[..., NOPE:], rotated_keys, preferred_element_type=jnp.float32
        )
    ) * scale
    allowed = key_pos[None, :] <= query_pos[:, None]
    scores = jnp.where(allowed[None], scores, -jnp.inf)
    block_max = jnp.max(scores, -1)
    weights = jnp.exp(scores - block_max[..., None])
    block_sum = jnp.sum(weights, -1)
    attended = jnp.einsum(
        "hqk,khd->qhd",
        weights.astype(jnp.bfloat16),
        keyvals[..., NOPE:],
        preferred_element_type=jnp.float32,
    ).astype(jnp.bfloat16)
    return (block_max.T, block_sum.T, attended)


def merge_block(carried, stats):
    running_max, running_sum, running_acc = carried
    block_max, block_sum, attended = stats
    new_max = jnp.maximum(running_max, block_max)
    old_weight = jnp.exp(running_max - new_max)
    new_weight = jnp.exp(block_max - new_max)
    return (
        new_max,
        running_sum * old_weight + block_sum * new_weight,
        running_acc * old_weight[..., None] + attended.astype(jnp.float32) * new_weight[..., None],
    )


def body(
    q_latent,
    kv_latent,
    rope_key,
    q_gain,
    kv_gain,
    w_query,
    w_keyval,
    w_output,
    moe_input,
    moe_gain,
    routes,
    route_weight,
    expert_gate,
    expert_up,
    expert_down,
    shared_gate,
    shared_up,
    shared_down,
):
    row_count = q_latent.shape[0]
    own_index = lax.axis_index("ep")
    ep_count = lax.axis_size("ep")
    tp_count = lax.axis_size("tp")
    positions = own_index * row_count + jnp.arange(row_count, dtype=jnp.int32)
    cosine_table, sine_table = rotary_tables(positions)
    q_normed = rms_scale(q_latent, q_gain)
    kv_normed = rms_scale(kv_latent, kv_gain)
    key_rotated = rotate(rope_key.astype(jnp.float32), cosine_table, sine_table).astype(
        jnp.bfloat16
    )
    heads_local = w_query.shape[1] // (NOPE + ROPE_DIM)
    projected = jnp.dot(q_normed, w_query, preferred_element_type=jnp.float32)
    projected = projected.reshape(row_count, heads_local, NOPE + ROPE_DIM)
    queries = jnp.concatenate(
        [
            projected[..., :NOPE],
            rotate(projected[..., NOPE:], cosine_table[:, None, :], sine_table[:, None, :]),
        ],
        -1,
    ).astype(jnp.bfloat16)

    def expand_keys(latent_rows):
        expanded = jnp.dot(latent_rows, w_keyval, preferred_element_type=jnp.float32).astype(
            jnp.bfloat16
        )
        return expanded.reshape(latent_rows.shape[0], heads_local, NOPE + VDIM)

    initial = (
        jnp.full((row_count, heads_local), floor_value, jnp.float32),
        jnp.zeros((row_count, heads_local), jnp.float32),
        jnp.zeros((row_count, heads_local, VDIM), jnp.float32),
    )
    carried = initial
    latent_piece = lax.all_gather(kv_normed, "ep", axis=0, tiled=True)
    rotated_piece = lax.all_gather(key_rotated, "ep", axis=0, tiled=True)
    block_count = latent_piece.shape[0] // row_count

    def visit_block(inner, offset):

        def live(current):
            latent_rows = lax.dynamic_slice_in_dim(latent_piece, offset * row_count, row_count, 0)
            rotated_rows = lax.dynamic_slice_in_dim(rotated_piece, offset * row_count, row_count, 0)
            key_pos = offset * row_count + jnp.arange(row_count, dtype=jnp.int32)
            stats = block_stats(queries, positions, expand_keys(latent_rows), rotated_rows, key_pos)
            return merge_block(current, stats)

        def skipped(current):
            return current

        return (lax.cond(offset <= own_index, live, skipped, inner), None)

    carried, unused = lax.scan(visit_block, carried, jnp.arange(block_count, dtype=jnp.int32))
    running_max, running_sum, running_acc = carried
    heads_out = (
        (running_acc / running_sum[..., None])
        .astype(jnp.bfloat16)
        .reshape(row_count, heads_local * VDIM)
    )
    mixed = jnp.dot(
        lax.all_gather(heads_out, "tp", axis=1, tiled=True),
        w_output,
        preferred_element_type=jnp.float32,
    )
    mixed = mixed.astype(jnp.bfloat16)
    width = moe_input.shape[1]
    top_count = routes.shape[1]
    local_experts = expert_gate.shape[0]
    expert_count = local_experts * ep_count
    capacity = max(2, 3 * MOE_DEV * top_count // (2 * expert_count))
    normed = layer_scale(moe_input, moe_gain)
    entries = routes.reshape(tp_count, MOE_DEV * top_count)
    onehot = (entries[..., None] == jnp.arange(expert_count, dtype=jnp.int32)).astype(jnp.int32)
    earlier = jnp.cumsum(onehot, 1) - onehot
    rank_in = jnp.sum(earlier * onehot, -1)
    block_ids = jnp.arange(tp_count, dtype=jnp.int32)[:, None]
    slot_of = ((entries * tp_count + block_ids) * capacity + rank_in).reshape(-1, top_count)
    token_ids = jnp.arange(tp_count * MOE_DEV * top_count, dtype=jnp.int32) // top_count
    slot_token = (
        jnp.full((expert_count * tp_count * capacity,), -1, jnp.int32)
        .at[slot_of.reshape(-1)]
        .set(token_ids)
    )
    outgoing = jnp.where(
        (slot_token >= 0)[:, None], normed[jnp.maximum(slot_token, 0)], jnp.zeros((), jnp.bfloat16)
    )
    outgoing = outgoing.reshape(ep_count, local_experts, tp_count, capacity, width)
    arrived = lax.all_to_all(outgoing, "ep", split_axis=0, concat_axis=0, tiled=True)
    slot_rows = arrived.shape[3]
    inputs = arrived[:, 0].reshape(-1, width)
    hidden = jax.nn.silu(jnp.dot(inputs, expert_gate[0], preferred_element_type=jnp.float32))
    hidden = (hidden * jnp.dot(inputs, expert_up[0], preferred_element_type=jnp.float32)).astype(
        jnp.bfloat16
    )
    output = jnp.dot(hidden, expert_down[0], preferred_element_type=jnp.float32)
    results = [output.astype(jnp.bfloat16).reshape(ep_count, tp_count, slot_rows, width)]
    partial_value = jnp.stack(results, 1)
    shared_hidden = jax.nn.silu(jnp.dot(normed, shared_gate, preferred_element_type=jnp.float32))
    shared_hidden = (
        shared_hidden * jnp.dot(normed, shared_up, preferred_element_type=jnp.float32)
    ).astype(jnp.bfloat16)
    shared_part = jnp.dot(shared_hidden, shared_down, preferred_element_type=jnp.float32).astype(
        jnp.bfloat16
    )
    slot_total, shared_total = (
        lax.psum_scatter(
            partial_value.astype(jnp.float32).astype(jnp.bfloat16),
            "tp",
            scatter_dimension=2,
            tiled=True,
        ).astype(jnp.float32),
        lax.psum_scatter(
            shared_part.astype(jnp.float32)
            .reshape(1, 1, tp_count, MOE_DEV, width)
            .astype(jnp.bfloat16),
            "tp",
            scatter_dimension=2,
            tiled=True,
        ).astype(jnp.float32),
    )
    arrived_sums = lax.all_to_all(
        slot_total.astype(jnp.bfloat16), "ep", split_axis=0, concat_axis=0, tiled=True
    ).astype(slot_total.dtype)
    own_block = lax.axis_index("tp")
    own_entries = lax.dynamic_slice_in_dim(routes, own_block * MOE_DEV, MOE_DEV, 0)
    own_rank = lax.dynamic_slice_in_dim(
        rank_in.reshape(-1, top_count), own_block * MOE_DEV, MOE_DEV, 0
    )
    own_weight = lax.dynamic_slice_in_dim(route_weight, own_block * MOE_DEV, MOE_DEV, 0)
    picked = arrived_sums.reshape(-1, width)[own_entries * capacity + own_rank]
    moe_out = (
        jnp.sum(own_weight[..., None] * picked, 1) + shared_total.reshape(MOE_DEV, width)
    ).astype(jnp.bfloat16)
    return (mixed, moe_out)


LANES = 128
LOG2E = 1.4426950408889634
MESH = pl.DeviceIdType.MESH


class Refs:
    pass


def fused_kernel(names, *refs):
    r = Refs()
    for name, ref in zip(names, refs):
        setattr(r, name, ref)
    f32, bf16 = jnp.float32, jnp.bfloat16
    e = lax.axis_index("ep")
    t = lax.axis_index("tp")
    c = t % 2
    d = t // 2
    ex, ey = e % 2, e // 2
    partner = (e, t + 1 - 2 * c)
    rows = r.kv_hbm.shape[0]
    half = rows // 2
    tile = rows // 4
    eighth = rows // 8
    latent = r.kv_hbm.shape[1]
    heads = r.k_all.shape[0]
    width = r.moe_hbm.shape[1]
    slots = r.xs.shape[1] // 2
    side = r.nrm.shape[1]
    depths = side // MOE_DEV
    capacity = slots // depths
    factor = float(NOPE + ROPE_DIM) ** (-0.5) * LOG2E
    halfway = ROPE_DIM // 2

    def ep_of(k):
        return ((ey + k // 2) % 2) * 2 + (ex + k % 2) % 2

    def rel_of(source):
        return ((source // 2 + ey) % 2) * 2 + (source % 2 + ex) % 2

    def remote(src, dst, send, recv, device):
        return pltpu.make_async_remote_copy(
            src_ref=src, dst_ref=dst, send_sem=send, recv_sem=recv,
            device_id=device, device_id_type=MESH,
        )

    loads = {}

    def load(name, src, dst, sem):
        copy = pltpu.make_async_copy(src, dst, r.ld.at[sem])
        copy.start()
        loads[name] = copy

    load("kv", r.kv_hbm, r.kv_raw, 0)
    load("table", r.table_hbm.at[pl.ds(pl.multiple_of(e * tile, tile), tile)], r.table, 1)
    for q in range(2):
        for j in range(depths):
            start = (2 * j + (c + q) % 2) * MOE_DEV
            load(
                f"moe{q}{j}",
                r.moe_hbm.at[pl.ds(pl.multiple_of(start, MOE_DEV), MOE_DEV)],
                r.nrm.at[q, pl.ds(j * MOE_DEV, MOE_DEV)],
                2 + q * depths + j,
            )
    first = 2 + 2 * depths
    load("q", r.q_hbm, r.q_raw, first)
    load("sg", r.sg_hbm, r.sg, first + 1)
    load("su", r.su_hbm, r.su, first + 2)
    load("sd", r.sd_hbm, r.sd, first + 3)
    load("eg", r.eg_hbm.at[0], r.eg, first + 4)
    load("eu", r.eu_hbm.at[0], r.eu, first + 5)
    load("ed", r.ed_hbm.at[0], r.ed, first + 6)
    load("wo", r.wo_hbm, r.wo, first + 7)

    barrier = pltpu.get_barrier_semaphore()
    peers = [partner] + [(ep_of(k), t) for k in (1, 2, 3)]
    peers += [(e, ((d + j) % depths) * 2 + c) for j in range(1, depths)]
    for peer in peers:
        pl.semaphore_signal(barrier, inc=1, device_id=peer, device_id_type=MESH)

    lane = lax.broadcasted_iota(jnp.int32, (tile, LANES), 1)
    low = (lane >= NOPE) & (lane < NOPE + halfway)
    high = (lane >= NOPE + halfway) & (lane < NOPE + ROPE_DIM)

    def rotated(values, cosine, sine):
        swapped = jnp.where(
            lane < NOPE + halfway,
            pltpu.roll(values, LANES - halfway, 1),
            pltpu.roll(values, halfway, 1),
        )
        return values * cosine + swapped * sine

    loads["table"].wait()
    for i in range(4):
        turned = pltpu.roll(r.table[...], (NOPE - ROPE_DIM * i) % LANES, 1)
        later = pltpu.roll(turned, halfway, 1)
        sooner = pltpu.roll(turned, LANES - halfway, 1)
        here = pl.ds(i * tile, tile)
        r.cosine[here, :] = jnp.where(
            lane < NOPE, 1.0, jnp.where(low, turned, jnp.where(high, later, 0.0))
        )
        r.sine[here, :] = jnp.where(low, -sooner, jnp.where(high, turned, 0.0))

    place = (
        lax.broadcasted_iota(jnp.int32, (ROPE_DIM, LANES), 0) + NOPE
        == lax.broadcasted_iota(jnp.int32, (ROPE_DIM, LANES), 1)
    ).astype(f32).astype(bf16)

    loads["kv"].wait()
    packed = [jnp.zeros((eighth, LANES), f32) for _ in range(2)]
    for i in range(4):
        here = pl.ds(i * tile, tile)
        values = r.kv_raw[here, :].astype(f32)
        scale = lax.rsqrt(jnp.mean(values * values, -1, keepdims=True) + norm_eps)
        r.kvs[0, here, :] = (values * scale * r.kv_gain[...]).astype(bf16)
        straight = jnp.dot(r.rope[here, :], place, preferred_element_type=f32)
        turned = rotated(straight, r.cosine[here, :], r.sine[here, :])
        for part in range(2):
            g = 2 * (i % 2) + part
            piece = turned[part * eighth : (part + 1) * eighth]
            packed[i // 2] += pltpu.roll(piece, (ROPE_DIM * g - NOPE) % LANES, 1)
    for h in range(2):
        r.ropes[0, h] = packed[h].astype(bf16)

    pl.semaphore_wait(barrier, len(peers))

    own_half = pl.ds(pl.multiple_of(c * half, half), half)

    def pack_copies(k):
        device = (ep_of(k), t)
        return [
            remote(r.kvs.at[0, own_half], r.kvs.at[k, own_half],
                   r.pk_s.at[k - 1, 0], r.pk_r.at[k - 1, 0], device),
            remote(r.ropes.at[0, c], r.ropes.at[k, c],
                   r.pk_s.at[k - 1, 1], r.pk_r.at[k - 1, 1], device),
        ]

    def pack_forwards(k):
        return [
            remote(r.kvs.at[k, own_half], r.kvs.at[k, own_half],
                   r.pf_s.at[k - 1, 0], r.pf_r.at[k - 1, 0], partner),
            remote(r.ropes.at[k, c], r.ropes.at[k, c],
                   r.pf_s.at[k - 1, 1], r.pf_r.at[k - 1, 1], partner),
        ]

    for k in (3, 2, 1):

        @pl.when(ep_of(k) > e)
        def _(k=k):
            for copy in pack_copies(k):
                copy.start()

    for q in range(2):
        for j in range(depths):
            loads[f"moe{q}{j}"].wait()

    chunk = 16

    def norm_rows(i, _):
        q = i // (side // chunk)
        here = pl.ds(pl.multiple_of((i % (side // chunk)) * chunk, chunk), chunk)
        values = r.nrm[q, here, :].astype(f32)
        centred = values - jnp.mean(values, -1, keepdims=True)
        scale = lax.rsqrt(jnp.mean(centred * centred, -1, keepdims=True) + layer_eps)
        r.nrm[q, here, :] = (centred * scale * r.moe_gain[...]).astype(bf16)
        return 0

    lax.fori_loop(0, 2 * side // chunk, norm_rows, 0)

    row_id = lax.broadcasted_iota(jnp.int32, (side, side), 0)
    col_id = lax.broadcasted_iota(jnp.int32, (side, side), 1)
    earlier = (
        (col_id < row_id) & (col_id // MOE_DEV == row_id // MOE_DEV)
    ).astype(f32).astype(bf16)

    def gather_rows(ref, q):
        return jnp.concatenate(
            [
                ref[pl.ds(pl.multiple_of((2 * j + (c + q) % 2) * MOE_DEV, MOE_DEV), MOE_DEV), :]
                for j in range(depths)
            ],
            0,
        )

    lane_side = lax.broadcasted_iota(jnp.int32, (side, LANES), 1)
    block_of = lax.broadcasted_iota(jnp.int32, (side, LANES), 0) // MOE_DEV
    for q in range(2):
        routes = gather_rows(r.routes, q)
        named = lane_side < 0
        for k in range(routes.shape[1]):
            named = named | (routes[:, k : k + 1] == lane_side)
        marked = named.astype(f32)
        rank = jnp.dot(earlier, marked.astype(bf16), preferred_element_type=f32)
        slot = jnp.where(named, rank + (block_of * capacity).astype(f32), -1.0)
        for k in (3, 2, 1, 0) if q == 0 else (0,):
            target = ep_of(k)
            mine = jnp.sum(jnp.where(lane_side == target, slot, 0.0), -1, keepdims=True)
            onehot = (mine == lane_side.astype(f32)).astype(f32)
            if q == 0:
                r.onehot[k] = onehot.astype(bf16)
            picked = jnp.dot(
                onehot.T.astype(bf16), r.nrm[q], preferred_element_type=f32
            )[:slots].astype(bf16)
            if k == 0:
                r.xs[0, q * slots : (q + 1) * slots, :] = picked
            else:
                r.snd[k - 1] = picked
                slot_copy = remote(
                    r.snd.at[k - 1], r.xs.at[k, pl.ds(0, slots)],
                    r.sl_s.at[k - 1], r.sl_r.at[k - 1], (target, t),
                )
                slot_copy.start()

    def slot_sends(k):
        return remote(
            r.snd.at[k - 1], r.xs.at[k, pl.ds(0, slots)],
            r.sl_s.at[k - 1], r.sl_r.at[k - 1], (ep_of(k), t),
        )

    def slot_forward(k):
        return remote(
            r.xs.at[k, pl.ds(0, slots)], r.xs.at[k, pl.ds(slots, slots)],
            r.sf_s.at[k - 1], r.sf_r.at[k - 1], partner,
        )

    def silu(values):
        return values / (1.0 + jnp.exp(-values))

    for name in ("sg", "su", "sd"):
        loads[name].wait()
    for q in range(2):
        inputs = r.nrm[q]
        hidden = silu(jnp.dot(inputs, r.sg[...], preferred_element_type=f32))
        hidden = (hidden * jnp.dot(inputs, r.su[...], preferred_element_type=f32)).astype(bf16)
        r.shared[q] = jnp.dot(hidden, r.sd[...], preferred_element_type=f32).astype(bf16)
    shared_copy = remote(r.shared.at[1], r.shared.at[2], r.sh_s, r.sh_r, partner)
    shared_copy.start()

    loads["q"].wait()

    def project(i, _):
        here = pl.ds(pl.multiple_of(i * tile, tile), tile)
        values = r.q_raw[here, :].astype(f32)
        scale = lax.rsqrt(jnp.mean(values * values, -1, keepdims=True) + norm_eps)
        normed = (values * scale * r.q_gain[...]).astype(bf16)
        projected = jnp.dot(normed, r.wq[...], preferred_element_type=f32)
        for head in range(heads):
            straight = projected[:, head * LANES : (head + 1) * LANES]
            r.q_all[head, here, :] = rotated(
                straight, r.cosine[here, :], r.sine[here, :]
            ).astype(bf16)
        return 0

    lax.fori_loop(0, 4, project, 0)

    lane_half = lax.broadcasted_iota(jnp.int32, (half, LANES), 1)

    def expand(k):
        for h in range(2):
            source = r.ropes[k, h].astype(f32)
            pieces = [
                pltpu.roll(source, (NOPE - ROPE_DIM * g) % LANES, 1) for g in range(4)
            ]
            turned = jnp.concatenate(pieces, 0)
            turned = jnp.where(
                (lane_half >= NOPE) & (lane_half < NOPE + ROPE_DIM), turned, 0.0
            )
            product = jnp.dot(
                r.kvs[k, h * half : (h + 1) * half, :], r.wkv[...], preferred_element_type=f32
            )
            start = pl.ds(pl.multiple_of(k * rows + h * half, half), half)
            for head in range(heads):
                pair = product[:, head * LANES : (head + 1) * LANES]
                r.k_all[head, start, :] = jnp.where(lane_half < NOPE, pair, turned).astype(bf16)
                r.v_all[head, start, :] = jnp.where(lane_half == 0, 1.0, pair).astype(bf16)

    def attend(queries, carry, start, size, masked):
        scored = [
            lax.dot_general(
                queries[head],
                r.k_all[head, pl.ds(start, size), :],
                (((1,), (1,)), ((), ())),
                preferred_element_type=f32,
            )
            for head in range(heads)
        ]
        result = []
        for head in range(heads):
            scores = scored[head]
            old_max, acc = carry[head]
            if masked:
                row = lax.broadcasted_iota(jnp.int32, scores.shape, 0)
                column = lax.broadcasted_iota(jnp.int32, scores.shape, 1)
                scores = jnp.where(column <= row, scores, -jnp.inf)
            new_max = jnp.maximum(old_max, jnp.max(scores, -1, keepdims=True))
            weights = jnp.exp2((scores - new_max) * factor).astype(bf16)
            product = jnp.dot(
                weights, r.v_all[head, pl.ds(start, size), :], preferred_element_type=f32
            )
            result.append((new_max, acc * jnp.exp2((old_max - new_max) * factor) + product))
        return tuple(result)

    expand(0)

    def local_tile(i, _):
        here = pl.ds(pl.multiple_of(i * tile, tile), tile)
        queries = [r.q_all[head, here, :] for head in range(heads)]
        carry = tuple(
            (jnp.full((tile, 1), floor_value, f32), jnp.zeros((tile, LANES), f32))
            for head in range(heads)
        )
        carry = attend(queries, carry, pl.multiple_of(i * tile, tile), tile, True)
        carry = lax.fori_loop(
            0, i,
            lambda j, cc: attend(queries, cc, pl.multiple_of(j * tile, tile), tile, False),
            carry,
        )
        for head in range(heads):
            r.top[head, here, :] = jnp.broadcast_to(carry[head][0], (tile, LANES))
            r.acc[head, here, :] = carry[head][1]
        return 0

    lax.fori_loop(0, 4, local_tile, 0)

    for k in (1, 2, 3):

        @pl.when(ep_of(k) < e)
        def _(k=k):
            for copy, forward in zip(pack_copies(k), pack_forwards(k)):
                copy.wait_recv()
                forward.start()

    for k in (1, 2, 3):

        @pl.when(ep_of(k) < e)
        def _(k=k):
            for forward in pack_forwards(k):
                forward.wait_recv()
            expand(k)

    head_cols = heads * VDIM
    own_cols = pl.ds(pl.multiple_of(t * head_cols, head_cols), head_cols)

    def remote_tile(i, _):
        here = pl.ds(pl.multiple_of(i * tile, tile), tile)
        queries = [r.q_all[head, here, :] for head in range(heads)]
        carry = tuple(
            (r.top[head, here, :][:, :1], r.acc[head, here, :]) for head in range(heads)
        )
        carry = lax.fori_loop(
            0, e,
            lambda s, cc: attend(
                queries, cc, pl.multiple_of(rel_of(s) * rows, rows), rows, False
            ),
            carry,
        )
        outs = [acc[:, NOPE : NOPE + VDIM] / acc[:, :1] for _, acc in carry]
        r.mixers[here, own_cols] = jnp.concatenate(outs, -1).astype(bf16)
        return 0

    lax.fori_loop(0, 4, remote_tile, 0)

    def depth_of(j):
        return (d + j) % depths

    def head_copy(j):
        device = partner if j == 0 else (e, depth_of(j) * 2 + c)
        return remote(
            r.mixers.at[:, own_cols], r.mixers.at[:, own_cols],
            r.h_s.at[j], r.h_r.at[j], device,
        )

    def head_forward(j):
        source = ((d + depths - j) % depths) * 2 + c
        cols = pl.ds(pl.multiple_of(source * head_cols, head_cols), head_cols)
        return remote(
            r.mixers.at[:, cols], r.mixers.at[:, cols],
            r.hf_s.at[j - 1], r.hf_r.at[j - 1], partner,
        )

    for j in range(depths):
        head_copy(j).start()

    for k in (3, 2, 1):
        slot_sends(k).wait_recv()
        slot_forward(k).start()
    for name in ("eg", "eu", "ed"):
        loads[name].wait()

    def partial_copy(k):
        return remote(r.theirs.at[k], r.pair.at[k], r.ex_s.at[k], r.ex_r.at[k], partner)

    def return_copy(k):
        return remote(
            r.sums.at[k], r.back.at[k, pl.ds(0, slots)],
            r.rt_s.at[k - 1], r.rt_r.at[k - 1], (ep_of(k), t),
        )

    hidden_units = r.eg.shape[1]
    step = min(256, hidden_units)
    out_step = min(512, width)

    def run_expert(k):
        inputs = r.xs[k]
        hidden = []
        for n in range(0, hidden_units, step):
            gate = silu(jnp.dot(inputs, r.eg[:, n : n + step], preferred_element_type=f32))
            up = jnp.dot(inputs, r.eu[:, n : n + step], preferred_element_type=f32)
            hidden.append((gate * up).astype(bf16))
        hidden = jnp.concatenate(hidden, 1)
        for n in range(0, width, out_step):
            product = jnp.dot(
                hidden, r.ed[:, n : n + out_step], preferred_element_type=f32
            ).astype(bf16)
            r.ours[k, :, n : n + out_step] = product[:slots]
            r.theirs[k, :, n : n + out_step] = product[slots:]
        partial_copy(k).start()

    def sum_pair(k):
        partial_copy(k).wait_recv()
        return (r.ours[k].astype(f32) + r.pair[k].astype(f32)).astype(bf16)

    def routed(i, _):
        k = 3 - i
        slot_forward(k).wait_recv()
        run_expert(k)

        @pl.when(i > 0)
        def _():
            r.sums[k + 1] = sum_pair(k + 1)
            return_copy(k + 1).start()

        return 0

    r.back[:, slots:, :] = jnp.zeros((4, r.back.shape[1] - slots, width), bf16)
    lax.fori_loop(0, 3, routed, 0)
    run_expert(0)
    r.sums[1] = sum_pair(1)
    return_copy(1).start()
    r.back[0, :slots, :] = sum_pair(0)
    shared_copy.wait_recv()

    for k in (3, 2, 1):
        return_copy(k).wait_recv()
    routes = gather_rows(r.routes, 0)
    weight = gather_rows(r.route_weight, 0)
    factors = [
        jnp.sum(jnp.where(routes == ep_of(k), weight, 0.0), -1, keepdims=True) for k in range(4)
    ]
    for n in range(0, width, out_step):
        cols = slice(n, n + out_step)
        total = r.shared[0, :, cols].astype(f32) + r.shared[2, :, cols].astype(f32)
        for k in range(4):
            total = total + factors[k] * jnp.dot(
                r.onehot[k], r.back[k, :, cols], preferred_element_type=f32
            )
        r.zs[:, cols] = total.astype(bf16)

    def z_copy(j):
        there = depth_of(j)
        return remote(
            r.zs.at[pl.ds(pl.multiple_of(there * MOE_DEV, MOE_DEV), MOE_DEV)],
            r.zr.at[j - 1],
            r.z_s.at[j - 1], r.z_r.at[j - 1], (e, there * 2 + c),
        )

    for j in range(1, depths):
        z_copy(j).start()

    for j in range(1, depths):
        head_copy(j).wait_recv()
        head_forward(j).start()
    loads["wo"].wait()
    head_copy(0).wait_recv()
    for j in range(1, depths):
        head_forward(j).wait_recv()

    def mix(i, _):
        here = pl.ds(pl.multiple_of(i * tile, tile), tile)
        r.mixed[here, :] = jnp.dot(
            r.mixers[here, :], r.wo[...], preferred_element_type=f32
        ).astype(bf16)
        return 0

    lax.fori_loop(0, 4, mix, 0)

    final = r.zs[pl.ds(pl.multiple_of(d * MOE_DEV, MOE_DEV), MOE_DEV), :].astype(f32)
    for j in range(1, depths):
        z_copy(j).wait_recv()
        final = final + r.zr[j - 1].astype(f32)
    r.moe_out[...] = final.astype(bf16)

    for k in (1, 2, 3):

        @pl.when(ep_of(k) > e)
        def _(k=k):
            for copy in pack_copies(k):
                copy.wait_send()

        @pl.when(ep_of(k) < e)
        def _(k=k):
            for copy in pack_forwards(k):
                copy.wait_send()

        slot_sends(k).wait_send()
        slot_forward(k).wait_send()
        return_copy(k).wait_send()
    shared_copy.wait_send()
    for k in range(4):
        partial_copy(k).wait_send()
    head_copy(0).wait_send()
    for j in range(1, depths):
        head_copy(j).wait_send()
        head_forward(j).wait_send()
        z_copy(j).wait_send()


def rotary_constant(total, per_device):
    halfway = ROPE_DIM // 2
    inverse = (
        np.float32(rotary_base)
        ** (-(np.arange(halfway, dtype=np.float32) * np.float32(2.0) / np.float32(ROPE_DIM)))
    ).astype(np.float32)
    angles = (np.arange(total, dtype=np.float32)[:, None] * inverse[None, :]).astype(np.float32)
    angles = angles.astype(np.float64)
    both = np.concatenate([np.cos(angles), np.sin(angles)], 1).astype(np.float32)
    groups = both.reshape(-1, LANES // ROPE_DIM, per_device * ROPE_DIM // LANES, ROPE_DIM)
    return groups.transpose(0, 2, 1, 3).reshape(-1, LANES)


def fused_body(
    q_latent,
    kv_latent,
    rope_key,
    q_gain,
    kv_gain,
    w_query,
    w_keyval,
    w_output,
    moe_input,
    moe_gain,
    routes,
    route_weight,
    expert_gate,
    expert_up,
    expert_down,
    shared_gate,
    shared_up,
    shared_down,
):
    rows, qlat = q_latent.shape
    latent = kv_latent.shape[1]
    ep_count = lax.axis_size("ep")
    tp_count = lax.axis_size("tp")
    heads = w_query.shape[1] // (NOPE + ROPE_DIM)
    tokens, width = moe_input.shape
    side = tokens // 2
    depths = tp_count // 2
    hidden = expert_gate.shape[2]
    shared_hidden = shared_gate.shape[1]
    top = routes.shape[1]
    capacity = 3 * MOE_DEV * top // (2 * ep_count)
    slots = depths * capacity
    columns = w_output.shape[1]
    bf16, f32 = jnp.bfloat16, jnp.float32
    table = jnp.asarray(rotary_constant(rows * ep_count, rows))
    padded = jnp.pad(
        w_query.reshape(qlat, heads, NOPE + ROPE_DIM),
        ((0, 0), (0, 0), (0, LANES - NOPE - ROPE_DIM)),
    ).reshape(qlat, heads * LANES)
    hbm = pl.BlockSpec(memory_space=pltpu.HBM)
    vmem = pl.BlockSpec(memory_space=pltpu.VMEM)
    inputs = [
        ("q_hbm", q_latent, hbm),
        ("kv_hbm", kv_latent, hbm),
        ("table_hbm", table, hbm),
        ("moe_hbm", moe_input, hbm),
        ("eg_hbm", expert_gate, hbm),
        ("eu_hbm", expert_up, hbm),
        ("ed_hbm", expert_down, hbm),
        ("sg_hbm", shared_gate, hbm),
        ("su_hbm", shared_up, hbm),
        ("sd_hbm", shared_down, hbm),
        ("wo_hbm", w_output, hbm),
        ("rope", rope_key, vmem),
        ("q_gain", q_gain.reshape(1, -1), vmem),
        ("kv_gain", kv_gain.reshape(1, -1), vmem),
        ("wq", padded, vmem),
        ("wkv", w_keyval, vmem),
        ("moe_gain", moe_gain.reshape(1, -1), vmem),
        ("routes", routes, vmem),
        ("route_weight", route_weight, vmem),
    ]
    outputs = [("mixed", (rows, columns)), ("moe_out", (MOE_DEV, width))]
    dma = pltpu.SemaphoreType.DMA
    scratch = [
        ("kv_raw", pltpu.VMEM((rows, latent), bf16)),
        ("q_raw", pltpu.VMEM((rows, qlat), bf16)),
        ("table", pltpu.VMEM((rows // 4, LANES), f32)),
        ("cosine", pltpu.VMEM((rows, LANES), f32)),
        ("sine", pltpu.VMEM((rows, LANES), f32)),
        ("kvs", pltpu.VMEM((4, rows, latent), bf16)),
        ("ropes", pltpu.VMEM((4, 2, rows // 8, LANES), bf16)),
        ("nrm", pltpu.VMEM((2, side, width), bf16)),
        ("onehot", pltpu.VMEM((4, side, LANES), bf16)),
        ("snd", pltpu.VMEM((3, slots, width), bf16)),
        ("xs", pltpu.VMEM((4, 2 * slots, width), bf16)),
        ("shared", pltpu.VMEM((3, side, width), bf16)),
        ("q_all", pltpu.VMEM((heads, rows, LANES), bf16)),
        ("k_all", pltpu.VMEM((heads, 4 * rows, LANES), bf16)),
        ("v_all", pltpu.VMEM((heads, 4 * rows, LANES), bf16)),
        ("top", pltpu.VMEM((heads, rows, LANES), f32)),
        ("acc", pltpu.VMEM((heads, rows, LANES), f32)),
        ("mixers", pltpu.VMEM((rows, tp_count * heads * VDIM), bf16)),
        ("ours", pltpu.VMEM((4, slots, width), bf16)),
        ("theirs", pltpu.VMEM((4, slots, width), bf16)),
        ("pair", pltpu.VMEM((4, slots, width), bf16)),
        ("sums", pltpu.VMEM((4, slots, width), bf16)),
        ("back", pltpu.VMEM((4, LANES, width), bf16)),
        ("zs", pltpu.VMEM((side, width), bf16)),
        ("zr", pltpu.VMEM((depths - 1, MOE_DEV, width), bf16)),
        ("eg", pltpu.VMEM((width, hidden), bf16)),
        ("eu", pltpu.VMEM((width, hidden), bf16)),
        ("ed", pltpu.VMEM((hidden, width), bf16)),
        ("sg", pltpu.VMEM((width, shared_hidden), bf16)),
        ("su", pltpu.VMEM((width, shared_hidden), bf16)),
        ("sd", pltpu.VMEM((shared_hidden, width), bf16)),
        ("wo", pltpu.VMEM(w_output.shape, bf16)),
        ("ld", dma((10 + 2 * depths,))),
        ("pk_s", dma((3, 2))),
        ("pk_r", dma((3, 2))),
        ("pf_s", dma((3, 2))),
        ("pf_r", dma((3, 2))),
        ("sl_s", dma((3,))),
        ("sl_r", dma((3,))),
        ("sf_s", dma((3,))),
        ("sf_r", dma((3,))),
        ("sh_s", dma),
        ("sh_r", dma),
        ("ex_s", dma((4,))),
        ("ex_r", dma((4,))),
        ("rt_s", dma((3,))),
        ("rt_r", dma((3,))),
        ("h_s", dma((depths,))),
        ("h_r", dma((depths,))),
        ("hf_s", dma((depths - 1,))),
        ("hf_r", dma((depths - 1,))),
        ("z_s", dma((depths - 1,))),
        ("z_r", dma((depths - 1,))),
    ]
    names = [x[0] for x in inputs] + [x[0] for x in outputs] + [x[0] for x in scratch]
    mixed, moe_out = pl.pallas_call(
        lambda *refs: fused_kernel(names, *refs),
        out_shape=[jax.ShapeDtypeStruct(shape, bf16) for _, shape in outputs],
        in_specs=[spec for _, _, spec in inputs],
        out_specs=[vmem] * len(outputs),
        scratch_shapes=[spec for _, spec in scratch],
        compiler_params=pltpu.CompilerParams(
            collective_id=0,
            has_side_effects=True,
            vmem_limit_bytes=60 * 1024 * 1024,
        ),
        name="fused",
    )(*[value for _, value, _ in inputs])
    return (mixed, moe_out)


def solution(mesh):
    in_specs = (
        P("ep", None),
        P("ep", None),
        P("ep", None),
        P(),
        P(),
        P(None, "tp"),
        P(None, "tp"),
        P(None, "tp"),
        P("ep", None),
        P(),
        P("ep", None),
        P("ep", None),
        P("ep", None, "tp"),
        P("ep", None, "tp"),
        P("ep", "tp", None),
        P(None, "tp"),
        P(None, "tp"),
        P("tp", None),
    )
    out_specs = (P("ep", "tp"), P(("ep", "tp"), None))
    chosen = fused_body if mesh.shape["ep"] == 4 else body
    return jax.shard_map(
        chosen, mesh=mesh, in_specs=in_specs, out_specs=out_specs, check_vma=False
    )
```

profile of v0, /device:TPU:14, one launch (start us, length us, event | category | flops | bytes accessed | tf_op | source)
XLA Modules:
  0.0 88.0 jit_solution(12649130041092547897)
XLA Ops:
  0.6 1.5 %copy.23.refs_17_ = s32[256,2]{1,0:T(8,128)} copy(s32[256,2]{0,1:T(2,128)} %param.29) | data formatting | bytes 4096 | tf_op args[10]
  2.1 1.5 %copy.24.refs_18_ = f32[256,2]{1,0:T(8,128)} copy(f32[256,2]{0,1:T(2,128)} %param.30) | data formatting | bytes 4096 | tf_op args[11]
  3.6 1.7 %copy.22.refs_11_ = bf16[1024,32]{1,0:T(8,128)(2,1)} copy(bf16[1024,32]{0,1:T(8,128)(2,1)} %param.21) | data formatting | bytes 131072 | tf_op args[2]
  5.3 1.1 %copy.21 = bf16[512,2,96]{2,1,0:T(2,128)(2,1)S(1)} copy(bf16[512,2,96]{0,2,1:T(8,128)(2,1)} %bitcast.10) | data formatting | bytes 393216 | tf_op jit(solution)/shard_map/reshape | solution.py:820
  6.4 0.3 pad.4
  6.6 0.7 copy.27
  7.4 77.1 %fused.1 = (bf16[1024,256]{1,0:T(8,128)(2,1)}, bf16[32,2048]{1,0:T(8,128)(2,1)}) custom-call(bf16[1024,512]{1,0:T(8,128)(2,1)} %refs_0_.1, bf16[1024,256]{1,0:T(8,128)(2,1)} %refs_1_.1, f32[1024,128]{1,0:T(8,128)} %constant.5.clone.refs_2_, bf16[256,2048]{1,0:T(8,128)(2,1)} %refs_3_.1, bf16[1,2048,512]{2,1,0:T(8,128)(2,1)} %refs_4_.1, ...), custom_call_target="tpu_custom_call" | custom-call | tf_op jit(solution)/shard_map/fused/pallas_call | solution.py:904
  84.5 1.9 %copy.30 = bf16[1024,256]{1,0:T(8,128)(2,1)} copy(bf16[1024,256]{1,0:T(8,128)(2,1)} %get-tuple-element.4) | data formatting | bytes 1048576
  86.4 1.6 %copy.31 = bf16[32,2048]{1,0:T(8,128)(2,1)} copy(bf16[32,2048]{1,0:T(8,128)(2,1)} %get-tuple-element.5) | data formatting | bytes 262144
where the time goes:
time: 88.3 us; the launch traced here: 88 us
  Pallas kernels  77.1 us (87%)
  local copies, waits for them, and re-layouts  10.2 us (12%)
    pallas_call x1, Pallas kernels, fused_body(): pl.pallas_call(lambda *refs: fused_kernel(names, *refs), out_shape=[jax.S...  77.1 us
    unnamed x6, local copies, waits for them, and re-layouts  8.81 us

commit v1 on v0

--- a/solution.py
+++ b/solution.py
@@ -305,16 +305,14 @@
 
     load("kv", r.kv_hbm, r.kv_raw, 0)
     load("table", r.table_hbm.at[pl.ds(pl.multiple_of(e * tile, tile), tile)], r.table, 1)
-    for q in range(2):
-        for j in range(depths):
-            start = (2 * j + (c + q) % 2) * MOE_DEV
-            load(
-                f"moe{q}{j}",
-                r.moe_hbm.at[pl.ds(pl.multiple_of(start, MOE_DEV), MOE_DEV)],
-                r.nrm.at[q, pl.ds(j * MOE_DEV, MOE_DEV)],
-                2 + q * depths + j,
-            )
-    first = 2 + 2 * depths
+    for j in range(depths):
+        load(
+            f"moe{j}",
+            r.moe_hbm.at[pl.ds(pl.multiple_of((2 * j + c) * MOE_DEV, MOE_DEV), MOE_DEV)],
+            r.nrm.at[0, pl.ds(j * MOE_DEV, MOE_DEV)],
+            2 + j,
+        )
+    first = 2 + depths
     load("q", r.q_hbm, r.q_raw, first)
     load("sg", r.sg_hbm, r.sg, first + 1)
     load("su", r.su_hbm, r.su, first + 2)
@@ -353,6 +351,12 @@
         )
         r.sine[here, :] = jnp.where(low, -sooner, jnp.where(high, turned, 0.0))
 
+    r.tags[...] = jnp.zeros(r.tags.shape, f32)
+    top = r.routes_t.shape[0]
+    r.tags[:top, :] = r.routes_t[...].astype(f32)
+    r.tags[top : 2 * top, :] = r.weight_t[...]
+    r.tagged[...] = r.tags[...].T
+
     place = (
         lax.broadcasted_iota(jnp.int32, (ROPE_DIM, LANES), 0) + NOPE
         == lax.broadcasted_iota(jnp.int32, (ROPE_DIM, LANES), 1)
@@ -365,7 +369,10 @@
         values = r.kv_raw[here, :].astype(f32)
         scale = lax.rsqrt(jnp.mean(values * values, -1, keepdims=True) + norm_eps)
         r.kvs[0, here, :] = (values * scale * r.kv_gain[...]).astype(bf16)
-        straight = jnp.dot(r.rope[here, :], place, preferred_element_type=f32)
+        straight = lax.dot_general(
+            r.rope_t[:, i * tile : (i + 1) * tile], place,
+            (((0,), (0,)), ((), ())), preferred_element_type=f32,
+        )
         turned = rotated(straight, r.cosine[here, :], r.sine[here, :])
         for part in range(2):
             g = 2 * (i % 2) + part
@@ -402,22 +409,22 @@
             for copy in pack_copies(k):
                 copy.start()
 
-    for q in range(2):
-        for j in range(depths):
-            loads[f"moe{q}{j}"].wait()
+    for j in range(depths):
+        loads[f"moe{j}"].wait()
 
     chunk = 16
 
     def norm_rows(i, _):
-        q = i // (side // chunk)
-        here = pl.ds(pl.multiple_of((i % (side // chunk)) * chunk, chunk), chunk)
-        values = r.nrm[q, here, :].astype(f32)
+        here = pl.ds(pl.multiple_of(i * chunk, chunk), chunk)
+        values = r.nrm[0, here, :].astype(f32)
         centred = values - jnp.mean(values, -1, keepdims=True)
         scale = lax.rsqrt(jnp.mean(centred * centred, -1, keepdims=True) + layer_eps)
-        r.nrm[q, here, :] = (centred * scale * r.moe_gain[...]).astype(bf16)
+        r.nrm[0, here, :] = (centred * scale * r.moe_gain[...]).astype(bf16)
         return 0
 
-    lax.fori_loop(0, 2 * side // chunk, norm_rows, 0)
+    lax.fori_loop(0, side // chunk, norm_rows, 0, unroll=2)
+    rows_copy = remote(r.nrm.at[0], r.nrm.at[1], r.rc_s, r.rc_r, partner)
+    rows_copy.start()
 
     row_id = lax.broadcasted_iota(jnp.int32, (side, side), 0)
     col_id = lax.broadcasted_iota(jnp.int32, (side, side), 1)
@@ -425,10 +432,10 @@
         (col_id < row_id) & (col_id // MOE_DEV == row_id // MOE_DEV)
     ).astype(f32).astype(bf16)
 
-    def gather_rows(ref, q):
+    def gather_rows(q):
         return jnp.concatenate(
             [
-                ref[pl.ds(pl.multiple_of((2 * j + (c + q) % 2) * MOE_DEV, MOE_DEV), MOE_DEV), :]
+                r.tagged[pl.ds(pl.multiple_of((2 * j + (c + q) % 2) * MOE_DEV, MOE_DEV), MOE_DEV), :]
                 for j in range(depths)
             ],
             0,
@@ -436,39 +443,37 @@
 
     lane_side = lax.broadcasted_iota(jnp.int32, (side, LANES), 1)
     block_of = lax.broadcasted_iota(jnp.int32, (side, LANES), 0) // MOE_DEV
-    for q in range(2):
-        routes = gather_rows(r.routes, q)
-        named = lane_side < 0
-        for k in range(routes.shape[1]):
-            named = named | (routes[:, k : k + 1] == lane_side)
-        marked = named.astype(f32)
-        rank = jnp.dot(earlier, marked.astype(bf16), preferred_element_type=f32)
-        slot = jnp.where(named, rank + (block_of * capacity).astype(f32), -1.0)
-        for k in (3, 2, 1, 0) if q == 0 else (0,):
-            target = ep_of(k)
-            mine = jnp.sum(jnp.where(lane_side == target, slot, 0.0), -1, keepdims=True)
-            onehot = (mine == lane_side.astype(f32)).astype(f32)
-            if q == 0:
-                r.onehot[k] = onehot.astype(bf16)
-            picked = jnp.dot(
-                onehot.T.astype(bf16), r.nrm[q], preferred_element_type=f32
-            )[:slots].astype(bf16)
-            if k == 0:
-                r.xs[0, q * slots : (q + 1) * slots, :] = picked
-            else:
-                r.snd[k - 1] = picked
-                slot_copy = remote(
-                    r.snd.at[k - 1], r.xs.at[k, pl.ds(0, slots)],
-                    r.sl_s.at[k - 1], r.sl_r.at[k - 1], (target, t),
-                )
-                slot_copy.start()
-
     def slot_sends(k):
         return remote(
             r.snd.at[k - 1], r.xs.at[k, pl.ds(0, slots)],
             r.sl_s.at[k - 1], r.sl_r.at[k - 1], (ep_of(k), t),
         )
 
+    def slot_table(q):
+        tags = gather_rows(q)
+        named = lane_side < 0
+        for k in range(top):
+            named = named | (tags[:, k : k + 1] == lane_side.astype(f32))
+        rank = jnp.dot(
+            earlier, named.astype(f32).astype(bf16), preferred_element_type=f32
+        )
+        return jnp.where(named, rank + (block_of * capacity).astype(f32), -1.0)
+
+    def pick_rows(slot, q, k):
+        mine = jnp.sum(jnp.where(lane_side == ep_of(k), slot, 0.0), -1, keepdims=True)
+        onehot = (mine == lane_side.astype(f32)).astype(f32)
+        if q == 0:
+            r.onehot[k] = onehot.astype(bf16)
+        return jnp.dot(
+            onehot.T.astype(bf16), r.nrm[q], preferred_element_type=f32
+        )[:slots].astype(bf16)
+
+    table = slot_table(0)
+    for k in (3, 2, 1):
+        r.snd[k - 1] = pick_rows(table, 0, k)
+        slot_sends(k).start()
+    r.xs[0, :slots, :] = pick_rows(table, 0, 0)
+
     def slot_forward(k):
         return remote(
             r.xs.at[k, pl.ds(0, slots)], r.xs.at[k, pl.ds(slots, slots)],
@@ -481,6 +486,9 @@
     for name in ("sg", "su", "sd"):
         loads[name].wait()
     for q in range(2):
+        if q == 1:
+            rows_copy.wait_recv()
+            r.xs[0, slots:, :] = pick_rows(slot_table(1), 1, 0)
         inputs = r.nrm[q]
         hidden = silu(jnp.dot(inputs, r.sg[...], preferred_element_type=f32))
         hidden = (hidden * jnp.dot(inputs, r.su[...], preferred_element_type=f32)).astype(bf16)
@@ -488,6 +496,16 @@
     shared_copy = remote(r.shared.at[1], r.shared.at[2], r.sh_s, r.sh_r, partner)
     shared_copy.start()
 
+    spread_row = lax.broadcasted_iota(jnp.int32, (r.wq_t.shape[0], heads * LANES), 0)
+    spread_col = lax.broadcasted_iota(jnp.int32, (r.wq_t.shape[0], heads * LANES), 1)
+    in_head = spread_col % LANES
+    spread = (
+        (in_head < NOPE + ROPE_DIM)
+        & (spread_row == (spread_col // LANES) * (NOPE + ROPE_DIM) + in_head)
+    ).astype(f32).astype(bf16)
+    r.wq[...] = lax.dot_general(
+        r.wq_t[...], spread, (((0,), (0,)), ((), ())), preferred_element_type=f32
+    ).astype(bf16)
     loads["q"].wait()
 
     def project(i, _):
@@ -540,8 +558,8 @@
         for head in range(heads):
             scores = scored[head]
             old_max, acc = carry[head]
-            if masked:
-                row = lax.broadcasted_iota(jnp.int32, scores.shape, 0)
+            if masked is not None:
+                row = lax.broadcasted_iota(jnp.int32, scores.shape, 0) + masked
                 column = lax.broadcasted_iota(jnp.int32, scores.shape, 1)
                 scores = jnp.where(column <= row, scores, -jnp.inf)
             new_max = jnp.maximum(old_max, jnp.max(scores, -1, keepdims=True))
@@ -554,25 +572,17 @@
 
     expand(0)
 
-    def local_tile(i, _):
-        here = pl.ds(pl.multiple_of(i * tile, tile), tile)
+    for i in range(4):
+        here = slice(i * tile, (i + 1) * tile)
         queries = [r.q_all[head, here, :] for head in range(heads)]
         carry = tuple(
             (jnp.full((tile, 1), floor_value, f32), jnp.zeros((tile, LANES), f32))
             for head in range(heads)
         )
-        carry = attend(queries, carry, pl.multiple_of(i * tile, tile), tile, True)
-        carry = lax.fori_loop(
-            0, i,
-            lambda j, cc: attend(queries, cc, pl.multiple_of(j * tile, tile), tile, False),
-            carry,
-        )
+        carry = attend(queries, carry, 0, (i + 1) * tile, i * tile)
         for head in range(heads):
             r.top[head, here, :] = jnp.broadcast_to(carry[head][0], (tile, LANES))
             r.acc[head, here, :] = carry[head][1]
-        return 0
-
-    lax.fori_loop(0, 4, local_tile, 0)
 
     for k in (1, 2, 3):
 
@@ -602,25 +612,28 @@
         carry = lax.fori_loop(
             0, e,
             lambda s, cc: attend(
-                queries, cc, pl.multiple_of(rel_of(s) * rows, rows), rows, False
+                queries, cc, pl.multiple_of(rel_of(s) * rows, rows), rows, None
             ),
             carry,
         )
         outs = [acc[:, NOPE : NOPE + VDIM] / acc[:, :1] for _, acc in carry]
         r.mixers[here, own_cols] = jnp.concatenate(outs, -1).astype(bf16)
+        for j in (3, 1, 2, 0):
+            head_copy(i, j).start()
         return 0
-
-    lax.fori_loop(0, 4, remote_tile, 0)
 
     def depth_of(j):
         return (d + j) % depths
 
-    def head_copy(j):
+    def head_copy(i, j):
         device = partner if j == 0 else (e, depth_of(j) * 2 + c)
+        here = pl.ds(pl.multiple_of(i * tile, tile), tile)
         return remote(
-            r.mixers.at[:, own_cols], r.mixers.at[:, own_cols],
-            r.h_s.at[j], r.h_r.at[j], device,
-        )
+            r.mixers.at[here, own_cols], r.mixers.at[here, own_cols],
+            r.h_s.at[i, j], r.h_r.at[i, j], device,
+        )
+
+    lax.fori_loop(0, 4, remote_tile, 0)
 
     def head_forward(j):
         source = ((d + depths - j) % depths) * 2 + c
@@ -630,102 +643,129 @@
             r.hf_s.at[j - 1], r.hf_r.at[j - 1], partner,
         )
 
-    for j in range(depths):
-        head_copy(j).start()
-
     for k in (3, 2, 1):
         slot_sends(k).wait_recv()
         slot_forward(k).start()
     for name in ("eg", "eu", "ed"):
         loads[name].wait()
 
-    def partial_copy(k):
-        return remote(r.theirs.at[k], r.pair.at[k], r.ex_s.at[k], r.ex_r.at[k], partner)
-
-    def return_copy(k):
+    quarter = width // 4
+    chunks = [(0, 2 * quarter), (2 * quarter, quarter), (3 * quarter, quarter)]
+
+    def partial_copy(n, k):
+        cols = pl.ds(*chunks[n])
         return remote(
-            r.sums.at[k], r.back.at[k, pl.ds(0, slots)],
-            r.rt_s.at[k - 1], r.rt_r.at[k - 1], (ep_of(k), t),
+            r.theirs.at[k, :, cols], r.pair.at[k, :, cols],
+            r.ex_s.at[n, k], r.ex_r.at[n, k], partner,
+        )
+
+    def return_copy(n, k):
+        cols = pl.ds(*chunks[n])
+        return remote(
+            r.sums.at[k, pl.ds(0, slots), cols], r.back.at[k, pl.ds(0, slots), cols],
+            r.rt_s.at[n, k - 1], r.rt_r.at[n, k - 1], (ep_of(k), t),
         )
 
     hidden_units = r.eg.shape[1]
     step = min(256, hidden_units)
-    out_step = min(512, width)
-
-    def run_expert(k):
+
+    def expert_hidden(k):
         inputs = r.xs[k]
-        hidden = []
         for n in range(0, hidden_units, step):
             gate = silu(jnp.dot(inputs, r.eg[:, n : n + step], preferred_element_type=f32))
             up = jnp.dot(inputs, r.eu[:, n : n + step], preferred_element_type=f32)
-            hidden.append((gate * up).astype(bf16))
-        hidden = jnp.concatenate(hidden, 1)
-        for n in range(0, width, out_step):
+            r.hid[k, :, n : n + step] = (gate * up).astype(bf16)
+
+    def expert_down(n, k):
+        for start in range(chunks[n][0], sum(chunks[n]), quarter):
+            cols = slice(start, start + quarter)
             product = jnp.dot(
-                hidden, r.ed[:, n : n + out_step], preferred_element_type=f32
+                r.hid[k], r.ed[:, cols], preferred_element_type=f32
             ).astype(bf16)
-            r.ours[k, :, n : n + out_step] = product[:slots]
-            r.theirs[k, :, n : n + out_step] = product[slots:]
-        partial_copy(k).start()
-
-    def sum_pair(k):
-        partial_copy(k).wait_recv()
-        return (r.ours[k].astype(f32) + r.pair[k].astype(f32)).astype(bf16)
-
-    def routed(i, _):
+            r.ours[k, :, cols] = product[:slots]
+            r.theirs[k, :, cols] = product[slots:]
+        partial_copy(n, k).start()
+
+    def finish(n, k):
+        cols = slice(chunks[n][0], sum(chunks[n]))
+        partial_copy(n, k).wait_recv()
+        r.sums[k, :slots, cols] = (
+            r.ours[k, :, cols].astype(f32) + r.pair[k, :, cols].astype(f32)
+        ).astype(bf16)
+
+    def first_pass(i, _):
         k = 3 - i
-        slot_forward(k).wait_recv()
-        run_expert(k)
+
+        @pl.when(k > 0)
+        def _():
+            slot_forward(k).wait_recv()
+
+        expert_hidden(k)
+        expert_down(0, k)
 
         @pl.when(i > 0)
         def _():
-            r.sums[k + 1] = sum_pair(k + 1)
-            return_copy(k + 1).start()
+            finish(0, k + 1)
+            return_copy(0, k + 1).start()
 
         return 0
 
     r.back[:, slots:, :] = jnp.zeros((4, r.back.shape[1] - slots, width), bf16)
-    lax.fori_loop(0, 3, routed, 0)
-    run_expert(0)
-    r.sums[1] = sum_pair(1)
-    return_copy(1).start()
-    r.back[0, :slots, :] = sum_pair(0)
+    r.sums[0, slots:, :] = jnp.zeros((r.back.shape[1] - slots, width), bf16)
+    lax.fori_loop(0, 4, first_pass, 0)
+    for n in (1, 2):
+
+        def later_pass(i, _, n=n):
+            k = 3 - i
+            expert_down(n, k)
+
+            @pl.when(i == 0)
+            def _():
+                finish(n - 1, 0)
+
+            @pl.when(i > 0)
+            def _():
+                finish(n, k + 1)
+                return_copy(n, k + 1).start()
+
+            return 0
+
+        lax.fori_loop(0, 4, later_pass, 0)
+    finish(2, 0)
     shared_copy.wait_recv()
 
-    for k in (3, 2, 1):
-        return_copy(k).wait_recv()
-    routes = gather_rows(r.routes, 0)
-    weight = gather_rows(r.route_weight, 0)
+    tags = gather_rows(0)
+    routes, weight = tags[:, :top], tags[:, top : 2 * top]
     factors = [
-        jnp.sum(jnp.where(routes == ep_of(k), weight, 0.0), -1, keepdims=True) for k in range(4)
+        jnp.sum(
+            jnp.where(routes == ep_of(k).astype(f32), weight, 0.0), -1, keepdims=True
+        )
+        for k in range(4)
     ]
-    for n in range(0, width, out_step):
-        cols = slice(n, n + out_step)
-        total = r.shared[0, :, cols].astype(f32) + r.shared[2, :, cols].astype(f32)
-        for k in range(4):
-            total = total + factors[k] * jnp.dot(
-                r.onehot[k], r.back[k, :, cols], preferred_element_type=f32
-            )
-        r.zs[:, cols] = total.astype(bf16)
-
-    def z_copy(j):
+
+    def z_copy(n, j):
         there = depth_of(j)
+        cols = pl.ds(*chunks[n])
         return remote(
-            r.zs.at[pl.ds(pl.multiple_of(there * MOE_DEV, MOE_DEV), MOE_DEV)],
-            r.zr.at[j - 1],
-            r.z_s.at[j - 1], r.z_r.at[j - 1], (e, there * 2 + c),
-        )
-
-    for j in range(1, depths):
-        z_copy(j).start()
-
-    for j in range(1, depths):
-        head_copy(j).wait_recv()
-        head_forward(j).start()
-    loads["wo"].wait()
-    head_copy(0).wait_recv()
-    for j in range(1, depths):
-        head_forward(j).wait_recv()
+            r.zs.at[pl.ds(pl.multiple_of(there * MOE_DEV, MOE_DEV), MOE_DEV), cols],
+            r.zr.at[j - 1, :, cols],
+            r.z_s.at[n, j - 1], r.z_r.at[n, j - 1], (e, there * 2 + c),
+        )
+
+    def combine(n):
+        for k in (3, 2, 1):
+            return_copy(n, k).wait_recv()
+        for start in range(chunks[n][0], sum(chunks[n]), quarter):
+            cols = slice(start, start + quarter)
+            total = r.shared[0, :, cols].astype(f32) + r.shared[2, :, cols].astype(f32)
+            for k in range(4):
+                source = r.back if k > 0 else r.sums
+                total = total + factors[k] * jnp.dot(
+                    r.onehot[k], source[k, :, cols], preferred_element_type=f32
+                )
+            r.zs[:, cols] = total.astype(bf16)
+        for j in range(1, depths):
+            z_copy(n, j).start()
 
     def mix(i, _):
         here = pl.ds(pl.multiple_of(i * tile, tile), tile)
@@ -734,11 +774,24 @@
         ).astype(bf16)
         return 0
 
+    combine(0)
+    combine(1)
+    for j in range(1, depths):
+        for i in range(4):
+            head_copy(i, j).wait_recv()
+        head_forward(j).start()
+    combine(2)
+    loads["wo"].wait()
+    for i in range(4):
+        head_copy(i, 0).wait_recv()
+    for j in range(1, depths):
+        head_forward(j).wait_recv()
     lax.fori_loop(0, 4, mix, 0)
-
+    for n in range(len(chunks)):
+        for j in range(1, depths):
+            z_copy(n, j).wait_recv()
     final = r.zs[pl.ds(pl.multiple_of(d * MOE_DEV, MOE_DEV), MOE_DEV), :].astype(f32)
     for j in range(1, depths):
-        z_copy(j).wait_recv()
         final = final + r.zr[j - 1].astype(f32)
     r.moe_out[...] = final.astype(bf16)
 
@@ -756,15 +809,20 @@
 
         slot_sends(k).wait_send()
         slot_forward(k).wait_send()
-        return_copy(k).wait_send()
+        for n in range(len(chunks)):
+            return_copy(n, k).wait_send()
     shared_copy.wait_send()
+    rows_copy.wait_send()
     for k in range(4):
-        partial_copy(k).wait_send()
-    head_copy(0).wait_send()
+        for n in range(len(chunks)):
+            partial_copy(n, k).wait_send()
+    for j in range(depths):
+        for i in range(4):
+            head_copy(i, j).wait_send()
     for j in range(1, depths):
-        head_copy(j).wait_send()
         head_forward(j).wait_send()
-        z_copy(j).wait_send()
+        for n in range(len(chunks)):
+            z_copy(n, j).wait_send()
 
 
 def rotary_constant(total, per_device):
@@ -816,10 +874,6 @@
     columns = w_output.shape[1]
     bf16, f32 = jnp.bfloat16, jnp.float32
     table = jnp.asarray(rotary_constant(rows * ep_count, rows))
-    padded = jnp.pad(
-        w_query.reshape(qlat, heads, NOPE + ROPE_DIM),
-        ((0, 0), (0, 0), (0, LANES - NOPE - ROPE_DIM)),
-    ).reshape(qlat, heads * LANES)
     hbm = pl.BlockSpec(memory_space=pltpu.HBM)
     vmem = pl.BlockSpec(memory_space=pltpu.VMEM)
     inputs = [
@@ -834,14 +888,14 @@
         ("su_hbm", shared_up, hbm),
         ("sd_hbm", shared_down, hbm),
         ("wo_hbm", w_output, hbm),
-        ("rope", rope_key, vmem),
+        ("rope_t", rope_key.T, vmem),
         ("q_gain", q_gain.reshape(1, -1), vmem),
         ("kv_gain", kv_gain.reshape(1, -1), vmem),
-        ("wq", padded, vmem),
+        ("wq_t", w_query.T, vmem),
         ("wkv", w_keyval, vmem),
         ("moe_gain", moe_gain.reshape(1, -1), vmem),
-        ("routes", routes, vmem),
-        ("route_weight", route_weight, vmem),
+        ("routes_t", routes.T, vmem),
+        ("weight_t", route_weight.T, vmem),
     ]
     outputs = [("mixed", (rows, columns)), ("moe_out", (MOE_DEV, width))]
     dma = pltpu.SemaphoreType.DMA
@@ -849,6 +903,9 @@
         ("kv_raw", pltpu.VMEM((rows, latent), bf16)),
         ("q_raw", pltpu.VMEM((rows, qlat), bf16)),
         ("table", pltpu.VMEM((rows // 4, LANES), f32)),
+        ("tags", pltpu.VMEM((LANES, tokens), f32)),
+        ("tagged", pltpu.VMEM((tokens, LANES), f32)),
+        ("wq", pltpu.VMEM((qlat, heads * LANES), bf16)),
         ("cosine", pltpu.VMEM((rows, LANES), f32)),
         ("sine", pltpu.VMEM((rows, LANES), f32)),
         ("kvs", pltpu.VMEM((4, rows, latent), bf16)),
@@ -867,7 +924,8 @@
         ("ours", pltpu.VMEM((4, slots, width), bf16)),
         ("theirs", pltpu.VMEM((4, slots, width), bf16)),
         ("pair", pltpu.VMEM((4, slots, width), bf16)),
-        ("sums", pltpu.VMEM((4, slots, width), bf16)),
+        ("sums", pltpu.VMEM((4, LANES, width), bf16)),
+        ("hid", pltpu.VMEM((4, 2 * slots, hidden), bf16)),
         ("back", pltpu.VMEM((4, LANES, width), bf16)),
         ("zs", pltpu.VMEM((side, width), bf16)),
         ("zr", pltpu.VMEM((depths - 1, MOE_DEV, width), bf16)),
@@ -878,7 +936,7 @@
         ("su", pltpu.VMEM((width, shared_hidden), bf16)),
         ("sd", pltpu.VMEM((shared_hidden, width), bf16)),
         ("wo", pltpu.VMEM(w_output.shape, bf16)),
-        ("ld", dma((10 + 2 * depths,))),
+        ("ld", dma((10 + depths,))),
         ("pk_s", dma((3, 2))),
         ("pk_r", dma((3, 2))),
         ("pf_s", dma((3, 2))),
@@ -887,18 +945,20 @@
         ("sl_r", dma((3,))),
         ("sf_s", dma((3,))),
         ("sf_r", dma((3,))),
+        ("rc_s", dma),
+        ("rc_r", dma),
         ("sh_s", dma),
         ("sh_r", dma),
-        ("ex_s", dma((4,))),
-        ("ex_r", dma((4,))),
-        ("rt_s", dma((3,))),
-        ("rt_r", dma((3,))),
-        ("h_s", dma((depths,))),
-        ("h_r", dma((depths,))),
+        ("ex_s", dma((3, 4))),
+        ("ex_r", dma((3, 4))),
+        ("rt_s", dma((3, 3))),
+        ("rt_r", dma((3, 3))),
+        ("h_s", dma((4, depths))),
+        ("h_r", dma((4, depths))),
         ("hf_s", dma((depths - 1,))),
         ("hf_r", dma((depths - 1,))),
-        ("z_s", dma((depths - 1,))),
-        ("z_r", dma((depths - 1,))),
+        ("z_s", dma((3, depths - 1))),
+        ("z_r", dma((3, depths - 1))),
     ]
     names = [x[0] for x in inputs] + [x[0] for x in outputs] + [x[0] for x in scratch]
     mixed, moe_out = pl.pallas_call(

time: 88.3 us -> 74.6 us (0.84)
  the two profiles are of different devices: /device:TPU:14 before, /device:TPU:0 now
where the time goes in v1:
time: 74.6 us; the launch traced here: 73.8 us
  Pallas kernels  69.8 us (94%)
  local copies, waits for them, and re-layouts  3.44 us (5%)
    pallas_call x1, Pallas kernels, fused_body(): pl.pallas_call(lambda *refs: fused_kernel(names, *refs), out_shape=[jax.S...  69.8 us
    unnamed x2, local copies, waits for them, and re-layouts  3.44 us

profile of v1, /device:TPU:0, one launch (start us, length us, event | category | flops | bytes accessed | tf_op | source)
XLA Modules:
  0.0 73.8 jit_solution(583796552735024901)
XLA Ops:
  0.6 69.8 %fused.1 = (bf16[1024,256]{1,0:T(8,128)(2,1)}, bf16[32,2048]{1,0:T(8,128)(2,1)}) custom-call(bf16[1024,512]{1,0:T(8,128)(2,1)} %refs_0_.1, bf16[1024,256]{1,0:T(8,128)(2,1)} %refs_1_.1, f32[1024,128]{1,0:T(8,128)} %constant.2.clone.refs_2_, bf16[256,2048]{1,0:T(8,128)(2,1)} %refs_3_.1, bf16[1,2048,512]{2,1,0:T(8,128)(2,1)} %refs_4_.1, ...), custom_call_target="tpu_custom_call" | custom-call | tf_op jit(solution)/shard_map/fused/pallas_call | solution.py:964
  70.4 1.9 %copy.23 = bf16[1024,256]{1,0:T(8,128)(2,1)} copy(bf16[1024,256]{1,0:T(8,128)(2,1)} %get-tuple-element.4) | data formatting | bytes 1048576
  72.3 1.6 %copy.24 = bf16[32,2048]{1,0:T(8,128)(2,1)} copy(bf16[32,2048]{1,0:T(8,128)(2,1)} %get-tuple-element.5) | data formatting | bytes 262144

commit v2 on v1

--- a/solution.py
+++ b/solution.py
@@ -385,14 +385,41 @@
 
     own_half = pl.ds(pl.multiple_of(c * half, half), half)
 
+    kv_part, rope_part = half // depths, eighth // depths
+
+    def depth_of(j):
+        return (d + j) % depths
+
+    def z_peer(j):
+        return (e, depth_of(j) * 2 + c)
+
+    kv_quarter = pl.ds(pl.multiple_of(c * half + d * kv_part, kv_part), kv_part)
+    rope_quarter = pl.ds(pl.multiple_of(d * rope_part, rope_part), rope_part)
+
     def pack_copies(k):
         device = (ep_of(k), t)
+        kv_rows, rope_rows = (kv_quarter, rope_quarter) if k == 3 else (own_half, slice(None))
         return [
-            remote(r.kvs.at[0, own_half], r.kvs.at[k, own_half],
+            remote(r.kvs.at[0, kv_rows], r.kvs.at[k, kv_rows],
                    r.pk_s.at[k - 1, 0], r.pk_r.at[k - 1, 0], device),
-            remote(r.ropes.at[0, c], r.ropes.at[k, c],
+            remote(r.ropes.at[0, c, rope_rows], r.ropes.at[k, c, rope_rows],
                    r.pk_s.at[k - 1, 1], r.pk_r.at[k - 1, 1], device),
         ]
+
+    def pack_spreads(j):
+        return [
+            remote(r.kvs.at[3, kv_quarter], r.kvs.at[3, kv_quarter],
+                   r.ps_s.at[j - 1, 0], r.ps_r.at[j - 1, 0], z_peer(j)),
+            remote(r.ropes.at[3, c, rope_quarter], r.ropes.at[3, c, rope_quarter],
+                   r.ps_s.at[j - 1, 1], r.ps_r.at[j - 1, 1], z_peer(j)),
+        ]
+
+    def spread_packs():
+        for copy in pack_copies(3):
+            copy.wait_recv()
+        for j in range(1, depths):
+            for copy in pack_spreads(j):
+                copy.start()
 
     def pack_forwards(k):
         return [
@@ -443,11 +470,23 @@
 
     lane_side = lax.broadcasted_iota(jnp.int32, (side, LANES), 1)
     block_of = lax.broadcasted_iota(jnp.int32, (side, LANES), 0) // MOE_DEV
+    slot_cols = pl.ds(pl.multiple_of(d * (width // depths), width // depths), width // depths)
+
     def slot_sends(k):
+        cols = slot_cols if k == 3 else slice(None)
         return remote(
-            r.snd.at[k - 1], r.xs.at[k, pl.ds(0, slots)],
+            r.snd.at[k - 1, :, cols], r.xs.at[k, pl.ds(0, slots), cols],
             r.sl_s.at[k - 1], r.sl_r.at[k - 1], (ep_of(k), t),
         )
+
+    def slot_spread(j):
+        there = r.xs.at[3, pl.ds(0, slots), slot_cols]
+        return remote(there, there, r.ss_s.at[j - 1], r.ss_r.at[j - 1], z_peer(j))
+
+    def spread_slots():
+        slot_sends(3).wait_recv()
+        for j in range(1, depths):
+            slot_spread(j).start()
 
     def slot_table(q):
         tags = gather_rows(q)
@@ -483,19 +522,9 @@
     def silu(values):
         return values / (1.0 + jnp.exp(-values))
 
-    for name in ("sg", "su", "sd"):
-        loads[name].wait()
-    for q in range(2):
-        if q == 1:
-            rows_copy.wait_recv()
-            r.xs[0, slots:, :] = pick_rows(slot_table(1), 1, 0)
-        inputs = r.nrm[q]
-        hidden = silu(jnp.dot(inputs, r.sg[...], preferred_element_type=f32))
-        hidden = (hidden * jnp.dot(inputs, r.su[...], preferred_element_type=f32)).astype(bf16)
-        r.shared[q] = jnp.dot(hidden, r.sd[...], preferred_element_type=f32).astype(bf16)
-    shared_copy = remote(r.shared.at[1], r.shared.at[2], r.sh_s, r.sh_r, partner)
-    shared_copy.start()
-
+    rows_copy.wait_recv()
+    r.xs[0, slots:, :] = pick_rows(slot_table(1), 1, 0)
+    pl.when(ep_of(3) < e)(spread_packs)
     spread_row = lax.broadcasted_iota(jnp.int32, (r.wq_t.shape[0], heads * LANES), 0)
     spread_col = lax.broadcasted_iota(jnp.int32, (r.wq_t.shape[0], heads * LANES), 1)
     in_head = spread_col % LANES
@@ -584,7 +613,7 @@
             r.top[head, here, :] = jnp.broadcast_to(carry[head][0], (tile, LANES))
             r.acc[head, here, :] = carry[head][1]
 
-    for k in (1, 2, 3):
+    for k in (1, 2):
 
         @pl.when(ep_of(k) < e)
         def _(k=k):
@@ -592,7 +621,7 @@
                 copy.wait_recv()
                 forward.start()
 
-    for k in (1, 2, 3):
+    for k in (1, 2):
 
         @pl.when(ep_of(k) < e)
         def _(k=k):
@@ -603,37 +632,42 @@
     head_cols = heads * VDIM
     own_cols = pl.ds(pl.multiple_of(t * head_cols, head_cols), head_cols)
 
-    def remote_tile(i, _):
-        here = pl.ds(pl.multiple_of(i * tile, tile), tile)
-        queries = [r.q_all[head, here, :] for head in range(heads)]
-        carry = tuple(
-            (r.top[head, here, :][:, :1], r.acc[head, here, :]) for head in range(heads)
-        )
-        carry = lax.fori_loop(
-            0, e,
-            lambda s, cc: attend(
-                queries, cc, pl.multiple_of(rel_of(s) * rows, rows), rows, None
-            ),
-            carry,
-        )
-        outs = [acc[:, NOPE : NOPE + VDIM] / acc[:, :1] for _, acc in carry]
-        r.mixers[here, own_cols] = jnp.concatenate(outs, -1).astype(bf16)
-        for j in (3, 1, 2, 0):
-            head_copy(i, j).start()
-        return 0
-
-    def depth_of(j):
-        return (d + j) % depths
+    wide = rows // 2
+    outer = 1 - ((d + 1) // 2) % 2
+    z_pair = d + 1 - 2 * (d % 2)
+    z_cross = outer * (3 - z_pair) + (1 - outer) * (3 - d)
 
     def head_copy(i, j):
-        device = partner if j == 0 else (e, depth_of(j) * 2 + c)
-        here = pl.ds(pl.multiple_of(i * tile, tile), tile)
+        device = (partner, (e, z_pair * 2 + c), (e, z_cross * 2 + c))[j]
+        here = pl.ds(pl.multiple_of(i * wide, wide), wide)
         return remote(
             r.mixers.at[here, own_cols], r.mixers.at[here, own_cols],
-            r.h_s.at[i, j], r.h_r.at[i, j], device,
-        )
-
-    lax.fori_loop(0, 4, remote_tile, 0)
+            r.h_s.at[i, j], r.h_r.at[i, j + outer if j == 2 else j], device,
+        )
+
+    def head_cross(i, j):
+        here = pl.ds(pl.multiple_of(i * wide, wide), wide)
+        return remote(
+            r.mixers.at[here, own_cols], r.mixers.at[here, own_cols],
+            r.h_s.at[i, 2], r.h_r.at[i, 2 + j], (e, z_cross * 2 + c),
+        )
+
+    def head_relay(i, j):
+        source = ((3 - d, (9 - 3 * (d + 1)) % 4)[j]) * 2 + c
+        here = pl.ds(pl.multiple_of(i * wide, wide), wide)
+        cols = pl.ds(pl.multiple_of(source * head_cols, head_cols), head_cols)
+        return remote(
+            r.mixers.at[here, cols], r.mixers.at[here, cols],
+            r.h_s.at[i, 3 + j], r.h_r.at[i, 4 + j], (e, z_pair * 2 + c),
+        )
+
+    def relay_heads(first, last):
+        @pl.when(outer == 0)
+        def _():
+            for i in range(first, last):
+                for j in range(2):
+                    head_cross(i, j).wait_recv()
+                    head_relay(i, j).start()
 
     def head_forward(j):
         source = ((d + depths - j) % depths) * 2 + c
@@ -643,20 +677,84 @@
             r.hf_s.at[j - 1], r.hf_r.at[j - 1], partner,
         )
 
-    for k in (3, 2, 1):
-        slot_sends(k).wait_recv()
+    near_first = 1 + ey * (1 - ex)
+    near_count = (ex + ey + 1) // 2 + ex * ey
+    far_count = ey
+
+    def tile_state(i):
+        here = pl.ds(pl.multiple_of(i * wide, wide), wide)
+        queries = [r.q_all[head, here, :] for head in range(heads)]
+        carry = tuple(
+            (r.top[head, here, :][:, :1], r.acc[head, here, :]) for head in range(heads)
+        )
+        return here, queries, carry
+
+    def forward_far():
+        for j in range(1, depths):
+            for copy in pack_spreads(j):
+                copy.wait_recv()
+        for forward in pack_forwards(3):
+            forward.start()
+
+    def near_tile(i, _):
+        here, queries, carry = tile_state(i)
+        carry = lax.fori_loop(
+            0, near_count,
+            lambda s, cc: attend(
+                queries, cc, pl.multiple_of((near_first + s) * rows, rows), rows, None
+            ),
+            carry,
+        )
+        for head in range(heads):
+            r.top[head, here, :] = jnp.broadcast_to(carry[head][0], (wide, LANES))
+            r.acc[head, here, :] = carry[head][1]
+
+        pl.when((i == 0) & (ep_of(3) < e))(forward_far)
+        return 0
+
+    spread_slots()
+    lax.fori_loop(0, 2, near_tile, 0)
+
+    @pl.when(ep_of(3) < e)
+    def _():
+        for forward in pack_forwards(3):
+            forward.wait_recv()
+        expand(3)
+
+    def far_tile(i, _):
+        here, queries, carry = tile_state(i)
+        carry = lax.fori_loop(
+            0, far_count,
+            lambda s, cc: attend(queries, cc, 3 * rows, rows, None),
+            carry,
+        )
+        outs = [acc[:, NOPE : NOPE + VDIM] / acc[:, :1] for _, acc in carry]
+        r.mixers[here, own_cols] = jnp.concatenate(outs, -1).astype(bf16)
+        for j in (2, 1, 0):
+            head_copy(i, j).start()
+        return 0
+
+    lax.fori_loop(0, 2, far_tile, 0)
+
+    for k in (1, 2, 3):
+        if k == 3:
+            for j in range(1, depths):
+                slot_spread(j).wait_recv()
+        else:
+            slot_sends(k).wait_recv()
         slot_forward(k).start()
     for name in ("eg", "eu", "ed"):
         loads[name].wait()
 
     quarter = width // 4
-    chunks = [(0, 2 * quarter), (2 * quarter, quarter), (3 * quarter, quarter)]
+    chunks = [(n * quarter, quarter) for n in range(4)]
 
     def partial_copy(n, k):
         cols = pl.ds(*chunks[n])
+        at = (k if n == 0 else slice(None), slice(None), cols)
         return remote(
-            r.theirs.at[k, :, cols], r.pair.at[k, :, cols],
-            r.ex_s.at[n, k], r.ex_r.at[n, k], partner,
+            r.theirs.at[at], r.pair.at[at],
+            r.ex_s.at[n, k if n == 0 else 0], r.ex_r.at[n, k if n == 0 else 0], partner,
         )
 
     def return_copy(n, k):
@@ -684,17 +782,15 @@
             ).astype(bf16)
             r.ours[k, :, cols] = product[:slots]
             r.theirs[k, :, cols] = product[slots:]
-        partial_copy(n, k).start()
-
-    def finish(n, k):
+
+    def add_pair(n, k):
         cols = slice(chunks[n][0], sum(chunks[n]))
-        partial_copy(n, k).wait_recv()
         r.sums[k, :slots, cols] = (
             r.ours[k, :, cols].astype(f32) + r.pair[k, :, cols].astype(f32)
         ).astype(bf16)
 
     def first_pass(i, _):
-        k = 3 - i
+        k = (i + 1) % 4
 
         @pl.when(k > 0)
         def _():
@@ -702,36 +798,59 @@
 
         expert_hidden(k)
         expert_down(0, k)
+        partial_copy(0, k).start()
 
         @pl.when(i > 0)
         def _():
-            finish(0, k + 1)
-            return_copy(0, k + 1).start()
-
+            partial_copy(0, i).wait_recv()
+            add_pair(0, i)
+            return_copy(0, i).start()
+
+        pl.when(i == 2)(lambda: relay_heads(0, 1))
         return 0
 
     r.back[:, slots:, :] = jnp.zeros((4, r.back.shape[1] - slots, width), bf16)
     r.sums[0, slots:, :] = jnp.zeros((r.back.shape[1] - slots, width), bf16)
     lax.fori_loop(0, 4, first_pass, 0)
-    for n in (1, 2):
-
-        def later_pass(i, _, n=n):
-            k = 3 - i
+
+    def later_pass(n):
+        def one(k, _):
             expert_down(n, k)
-
-            @pl.when(i == 0)
-            def _():
-                finish(n - 1, 0)
-
-            @pl.when(i > 0)
-            def _():
-                finish(n, k + 1)
-                return_copy(n, k + 1).start()
-
             return 0
 
-        lax.fori_loop(0, 4, later_pass, 0)
-    finish(2, 0)
+        lax.fori_loop(0, 4, one, 0)
+        partial_copy(n, 0).start()
+
+    def later_sums(n):
+        partial_copy(n, 0).wait_recv()
+
+        def one(k, _):
+            add_pair(n, k)
+            return_copy(n, k).start()
+            return 0
+
+        lax.fori_loop(1, 4, one, 0)
+        add_pair(n, 0)
+
+    later_pass(1)
+    partial_copy(0, 0).wait_recv()
+    add_pair(0, 0)
+    later_pass(2)
+    later_sums(1)
+    relay_heads(1, 2)
+    later_pass(3)
+    later_sums(2)
+    later_sums(3)
+    for name in ("sg", "su", "sd"):
+        loads[name].wait()
+    for q in range(2):
+        inputs = r.nrm[q]
+        hidden = silu(jnp.dot(inputs, r.sg[...], preferred_element_type=f32))
+        hidden = (hidden * jnp.dot(inputs, r.su[...], preferred_element_type=f32)).astype(bf16)
+        r.shared[q] = jnp.dot(hidden, r.sd[...], preferred_element_type=f32).astype(bf16)
+    shared_copy = remote(r.shared.at[1], r.shared.at[2], r.sh_s, r.sh_r, partner)
+    shared_copy.start()
+
     shared_copy.wait_recv()
 
     tags = gather_rows(0)
@@ -776,13 +895,21 @@
 
     combine(0)
     combine(1)
+    combine(2)
+    for i in range(2):
+        head_copy(i, 1).wait_recv()
+
+    @pl.when(outer == 1)
+    def _():
+        for i in range(2):
+            for j in range(2):
+                head_relay(i, j).wait_recv()
+
     for j in range(1, depths):
-        for i in range(4):
-            head_copy(i, j).wait_recv()
         head_forward(j).start()
-    combine(2)
+    combine(3)
     loads["wo"].wait()
-    for i in range(4):
+    for i in range(2):
         head_copy(i, 0).wait_recv()
     for j in range(1, depths):
         head_forward(j).wait_recv()
@@ -806,6 +933,10 @@
         def _(k=k):
             for copy in pack_forwards(k):
                 copy.wait_send()
+            if k == 3:
+                for j in range(1, depths):
+                    for copy in pack_spreads(j):
+                        copy.wait_send()
 
         slot_sends(k).wait_send()
         slot_forward(k).wait_send()
@@ -814,12 +945,21 @@
     shared_copy.wait_send()
     rows_copy.wait_send()
     for k in range(4):
-        for n in range(len(chunks)):
-            partial_copy(n, k).wait_send()
-    for j in range(depths):
-        for i in range(4):
+        partial_copy(0, k).wait_send()
+    for n in range(1, len(chunks)):
+        partial_copy(n, 0).wait_send()
+    for i in range(2):
+        for j in range(3):
             head_copy(i, j).wait_send()
+
+    @pl.when(outer == 0)
+    def _():
+        for i in range(2):
+            for j in range(2):
+                head_relay(i, j).wait_send()
+
     for j in range(1, depths):
+        slot_spread(j).wait_send()
         head_forward(j).wait_send()
         for n in range(len(chunks)):
             z_copy(n, j).wait_send()
@@ -943,22 +1083,26 @@
         ("pf_r", dma((3, 2))),
         ("sl_s", dma((3,))),
         ("sl_r", dma((3,))),
+        ("ps_s", dma((depths - 1, 2))),
+        ("ps_r", dma((depths - 1, 2))),
+        ("ss_s", dma((depths - 1,))),
+        ("ss_r", dma((depths - 1,))),
         ("sf_s", dma((3,))),
         ("sf_r", dma((3,))),
         ("rc_s", dma),
         ("rc_r", dma),
         ("sh_s", dma),
         ("sh_r", dma),
-        ("ex_s", dma((3, 4))),
-        ("ex_r", dma((3, 4))),
-        ("rt_s", dma((3, 3))),
-        ("rt_r", dma((3, 3))),
-        ("h_s", dma((4, depths))),
-        ("h_r", dma((4, depths))),
+        ("ex_s", dma((4, 4))),
+        ("ex_r", dma((4, 4))),
+        ("rt_s", dma((4, 3))),
+        ("rt_r", dma((4, 3))),
+        ("h_s", dma((2, 5))),
+        ("h_r", dma((2, 6))),
         ("hf_s", dma((depths - 1,))),
         ("hf_r", dma((depths - 1,))),
-        ("z_s", dma((3, depths - 1))),
-        ("z_r", dma((3, depths - 1))),
+        ("z_s", dma((4, depths - 1))),
+        ("z_r", dma((4, depths - 1))),
     ]
     names = [x[0] for x in inputs] + [x[0] for x in outputs] + [x[0] for x in scratch]
     mixed, moe_out = pl.pallas_call(
@@ -999,7 +1143,7 @@
         P("tp", None),
     )
     out_specs = (P("ep", "tp"), P(("ep", "tp"), None))
-    chosen = fused_body if mesh.shape["ep"] == 4 else body
+    chosen = fused_body if (mesh.shape["ep"], mesh.shape["tp"]) == (4, 8) else body
     return jax.shard_map(
         chosen, mesh=mesh, in_specs=in_specs, out_specs=out_specs, check_vma=False
     )

time: 74.6 us -> 69.5 us (0.932)
  Pallas kernels: 69.8 us -> 65.2 us
    pallas_call x1, Pallas kernels: 69.8 us -> 65.2 us  [fused_body(): pl.pallas_call(lambda *refs: fused_kernel(names, *refs), out_shape=[jax.S...]
where the time goes in v2:
time: 69.5 us; the launch traced here: 69.3 us
  Pallas kernels  65.2 us (94%)
  local copies, waits for them, and re-layouts  3.44 us (5%)
    pallas_call x1, Pallas kernels, fused_body(): pl.pallas_call(lambda *refs: fused_kernel(names, *refs), out_shape=[jax.S...  65.2 us
    unnamed x2, local copies, waits for them, and re-layouts  3.44 us

profile of v2, /device:TPU:0, one launch (start us, length us, event | category | flops | bytes accessed | tf_op | source)
XLA Modules:
  0.0 69.3 jit_solution(1373071002771216537)
XLA Ops:
  0.6 65.2 %fused.1 = (bf16[1024,256]{1,0:T(8,128)(2,1)}, bf16[32,2048]{1,0:T(8,128)(2,1)}) custom-call(bf16[1024,512]{1,0:T(8,128)(2,1)} %refs_0_.1, bf16[1024,256]{1,0:T(8,128)(2,1)} %refs_1_.1, f32[1024,128]{1,0:T(8,128)} %constant.2.clone.refs_2_, bf16[256,2048]{1,0:T(8,128)(2,1)} %refs_3_.1, bf16[1,2048,512]{2,1,0:T(8,128)(2,1)} %refs_4_.1, ...), custom_call_target="tpu_custom_call" | custom-call | tf_op jit(solution)/shard_map/fused/pallas_call | solution.py:1108
  65.9 1.9 %copy.23 = bf16[1024,256]{1,0:T(8,128)(2,1)} copy(bf16[1024,256]{1,0:T(8,128)(2,1)} %get-tuple-element.4) | data formatting | bytes 1048576
  67.8 1.6 %copy.24 = bf16[32,2048]{1,0:T(8,128)(2,1)} copy(bf16[32,2048]{1,0:T(8,128)(2,1)} %get-tuple-element.5) | data formatting | bytes 262144

commit v3 on v2

--- a/solution.py
+++ b/solution.py
@@ -340,47 +340,42 @@
         )
         return values * cosine + swapped * sine
 
-    loads["table"].wait()
-    for i in range(4):
-        turned = pltpu.roll(r.table[...], (NOPE - ROPE_DIM * i) % LANES, 1)
-        later = pltpu.roll(turned, halfway, 1)
-        sooner = pltpu.roll(turned, LANES - halfway, 1)
-        here = pl.ds(i * tile, tile)
-        r.cosine[here, :] = jnp.where(
-            lane < NOPE, 1.0, jnp.where(low, turned, jnp.where(high, later, 0.0))
-        )
-        r.sine[here, :] = jnp.where(low, -sooner, jnp.where(high, turned, 0.0))
-
-    r.tags[...] = jnp.zeros(r.tags.shape, f32)
-    top = r.routes_t.shape[0]
-    r.tags[:top, :] = r.routes_t[...].astype(f32)
-    r.tags[top : 2 * top, :] = r.weight_t[...]
-    r.tagged[...] = r.tags[...].T
-
     place = (
         lax.broadcasted_iota(jnp.int32, (ROPE_DIM, LANES), 0) + NOPE
         == lax.broadcasted_iota(jnp.int32, (ROPE_DIM, LANES), 1)
     ).astype(f32).astype(bf16)
 
+    loads["table"].wait()
     loads["kv"].wait()
-    packed = [jnp.zeros((eighth, LANES), f32) for _ in range(2)]
-    for i in range(4):
-        here = pl.ds(i * tile, tile)
-        values = r.kv_raw[here, :].astype(f32)
-        scale = lax.rsqrt(jnp.mean(values * values, -1, keepdims=True) + norm_eps)
-        r.kvs[0, here, :] = (values * scale * r.kv_gain[...]).astype(bf16)
-        straight = lax.dot_general(
-            r.rope_t[:, i * tile : (i + 1) * tile], place,
-            (((0,), (0,)), ((), ())), preferred_element_type=f32,
-        )
-        turned = rotated(straight, r.cosine[here, :], r.sine[here, :])
-        for part in range(2):
-            g = 2 * (i % 2) + part
-            piece = turned[part * eighth : (part + 1) * eighth]
-            packed[i // 2] += pltpu.roll(piece, (ROPE_DIM * g - NOPE) % LANES, 1)
-    for h in range(2):
-        r.ropes[0, h] = packed[h].astype(bf16)
-
+
+    def key_half(h):
+        packed = jnp.zeros((eighth, LANES), f32)
+        for which in range(2):
+            i = 2 * h + which
+            here = pl.ds(pl.multiple_of(i * tile, tile), tile)
+            turned = pltpu.roll(r.table[...], (NOPE - ROPE_DIM * i + LANES) % LANES, 1)
+            later = pltpu.roll(turned, halfway, 1)
+            sooner = pltpu.roll(turned, LANES - halfway, 1)
+            cosine = jnp.where(
+                lane < NOPE, 1.0, jnp.where(low, turned, jnp.where(high, later, 0.0))
+            )
+            sine = jnp.where(low, -sooner, jnp.where(high, turned, 0.0))
+            r.cosine[here, :] = cosine
+            r.sine[here, :] = sine
+            values = r.kv_raw[here, :].astype(f32)
+            scale = lax.rsqrt(jnp.mean(values * values, -1, keepdims=True) + norm_eps)
+            r.kvs[0, here, :] = (values * scale * r.kv_gain[...]).astype(bf16)
+            straight = lax.dot_general(
+                r.rope_t[:, here], place, (((0,), (0,)), ((), ())), preferred_element_type=f32
+            )
+            turned = rotated(straight, cosine, sine)
+            for part in range(2):
+                piece = turned[part * eighth : (part + 1) * eighth]
+                shift = (ROPE_DIM * (2 * which + part) - NOPE) % LANES
+                packed += pltpu.roll(piece, shift, 1)
+        r.ropes[0, h] = packed.astype(bf16)
+
+    key_half(c)
     pl.semaphore_wait(barrier, len(peers))
 
     own_half = pl.ds(pl.multiple_of(c * half, half), half)
@@ -436,6 +431,8 @@
             for copy in pack_copies(k):
                 copy.start()
 
+    key_half(1 - c)
+
     for j in range(depths):
         loads[f"moe{j}"].wait()
 
@@ -452,6 +449,12 @@
     lax.fori_loop(0, side // chunk, norm_rows, 0, unroll=2)
     rows_copy = remote(r.nrm.at[0], r.nrm.at[1], r.rc_s, r.rc_r, partner)
     rows_copy.start()
+
+    r.tags[...] = jnp.zeros(r.tags.shape, f32)
+    top = r.routes_t.shape[0]
+    r.tags[:top, :] = r.routes_t[...].astype(f32)
+    r.tags[top : 2 * top, :] = r.weight_t[...]
+    r.tagged[...] = r.tags[...].T
 
     row_id = lax.broadcasted_iota(jnp.int32, (side, side), 0)
     col_id = lax.broadcasted_iota(jnp.int32, (side, side), 1)
@@ -747,7 +750,8 @@
         loads[name].wait()
 
     quarter = width // 4
-    chunks = [(n * quarter, quarter) for n in range(4)]
+    chunks = [(n * quarter, quarter) for n in range(3)]
+    chunks += [(3 * quarter, quarter // 2), (7 * quarter // 2, quarter // 2)]
 
     def partial_copy(n, k):
         cols = pl.ds(*chunks[n])
@@ -775,8 +779,8 @@
             r.hid[k, :, n : n + step] = (gate * up).astype(bf16)
 
     def expert_down(n, k):
-        for start in range(chunks[n][0], sum(chunks[n]), quarter):
-            cols = slice(start, start + quarter)
+        for start, size in chunks[n : n + 1]:
+            cols = slice(start, start + size)
             product = jnp.dot(
                 r.hid[k], r.ed[:, cols], preferred_element_type=f32
             ).astype(bf16)
@@ -840,7 +844,9 @@
     relay_heads(1, 2)
     later_pass(3)
     later_sums(2)
+    later_pass(4)
     later_sums(3)
+    later_sums(4)
     for name in ("sg", "su", "sd"):
         loads[name].wait()
     for q in range(2):
@@ -851,7 +857,6 @@
     shared_copy = remote(r.shared.at[1], r.shared.at[2], r.sh_s, r.sh_r, partner)
     shared_copy.start()
 
-    shared_copy.wait_recv()
 
     tags = gather_rows(0)
     routes, weight = tags[:, :top], tags[:, top : 2 * top]
@@ -874,8 +879,10 @@
     def combine(n):
         for k in (3, 2, 1):
             return_copy(n, k).wait_recv()
-        for start in range(chunks[n][0], sum(chunks[n]), quarter):
-            cols = slice(start, start + quarter)
+        if n == 0:
+            shared_copy.wait_recv()
+        for start, size in chunks[n : n + 1]:
+            cols = slice(start, start + size)
             total = r.shared[0, :, cols].astype(f32) + r.shared[2, :, cols].astype(f32)
             for k in range(4):
                 source = r.back if k > 0 else r.sums
@@ -908,6 +915,7 @@
     for j in range(1, depths):
         head_forward(j).start()
     combine(3)
+    combine(4)
     loads["wo"].wait()
     for i in range(2):
         head_copy(i, 0).wait_recv()
@@ -1093,16 +1101,16 @@
         ("rc_r", dma),
         ("sh_s", dma),
         ("sh_r", dma),
-        ("ex_s", dma((4, 4))),
-        ("ex_r", dma((4, 4))),
-        ("rt_s", dma((4, 3))),
-        ("rt_r", dma((4, 3))),
+        ("ex_s", dma((5, 4))),
+        ("ex_r", dma((5, 4))),
+        ("rt_s", dma((5, 3))),
+        ("rt_r", dma((5, 3))),
         ("h_s", dma((2, 5))),
         ("h_r", dma((2, 6))),
         ("hf_s", dma((depths - 1,))),
         ("hf_r", dma((depths - 1,))),
-        ("z_s", dma((4, depths - 1))),
-        ("z_r", dma((4, depths - 1))),
+        ("z_s", dma((5, depths - 1))),
+        ("z_r", dma((5, depths - 1))),
     ]
     names = [x[0] for x in inputs] + [x[0] for x in outputs] + [x[0] for x in scratch]
     mixed, moe_out = pl.pallas_call(

time: 69.5 us -> 68.6 us (0.987)
  Pallas kernels: 65.2 us -> 64.3 us
    pallas_call x1, Pallas kernels: 65.2 us -> 64.3 us  [fused_body(): pl.pallas_call(lambda *refs: fused_kernel(names, *refs), out_shape=[jax.S...]
where the time goes in v3:
time: 68.6 us; the launch traced here: 68.4 us
  Pallas kernels  64.3 us (94%)
  local copies, waits for them, and re-layouts  3.44 us (5%)
    pallas_call x1, Pallas kernels, fused_body(): pl.pallas_call(lambda *refs: fused_kernel(names, *refs), out_shape=[jax.S...  64.3 us
    unnamed x2, local copies, waits for them, and re-layouts  3.44 us

profile of v3, /device:TPU:0, one launch (start us, length us, event | category | flops | bytes accessed | tf_op | source)
XLA Modules:
  0.0 68.4 jit_solution(6833098675881684725)
XLA Ops:
  0.6 64.3 %fused.1 = (bf16[1024,256]{1,0:T(8,128)(2,1)}, bf16[32,2048]{1,0:T(8,128)(2,1)}) custom-call(bf16[1024,512]{1,0:T(8,128)(2,1)} %refs_0_.1, bf16[1024,256]{1,0:T(8,128)(2,1)} %refs_1_.1, f32[1024,128]{1,0:T(8,128)} %constant.2.clone.refs_2_, bf16[256,2048]{1,0:T(8,128)(2,1)} %refs_3_.1, bf16[1,2048,512]{2,1,0:T(8,128)(2,1)} %refs_4_.1, ...), custom_call_target="tpu_custom_call" | custom-call | tf_op jit(solution)/shard_map/fused/pallas_call | solution.py:1116
  65.0 1.9 %copy.23 = bf16[1024,256]{1,0:T(8,128)(2,1)} copy(bf16[1024,256]{1,0:T(8,128)(2,1)} %get-tuple-element.4) | data formatting | bytes 1048576
  66.9 1.6 %copy.24 = bf16[32,2048]{1,0:T(8,128)(2,1)} copy(bf16[32,2048]{1,0:T(8,128)(2,1)} %get-tuple-element.5) | data formatting | bytes 262144
